TPU v7x, 256 devices: a whole 4x4x8 slice. The times are simulated.
256 devices in a mesh: sp: 16 (over y, x), dp: 16 (over z, core).
Axes of the slice: x: 4, y: 4, z: 8, core: 2. Of those that a mesh axis runs over, the one named last changes fastest.
Arguments:
- tokens: bfloat16 [16, 6144, 2048], P('dp', 'sp'), may hold values from -6 to 6
- value_act: bfloat16 [16, 6144, 1024], P('dp', 'sp'), may hold values from -6 to 6
- gate_act: bfloat16 [16, 6144, 1024], P('dp', 'sp'), may hold values from -6 to 6
- cotangent: bfloat16 [16, 6144, 1024], P('dp', 'sp'), may hold values from -6 to 6
- value_weight: bfloat16 [2048, 1024], P('dp'), may hold values from -0.1875 to 0.1875
- gate_weight: bfloat16 [2048, 1024], P('dp'), may hold values from -0.1875 to 0.1875
- norm_gain: float32 [1024], replicated, may hold values from 0.1 to 1.9
- norm_bias: float32 [1024], replicated, may hold values from -3 to 3
- mix_weight: bfloat16 [16, 128, 128], replicated, may hold values from -0.5 to 0.5
- mix_bias: float32 [16, 128], replicated, may hold values from 0.1 to 1.9
Outputs:
- tokens_grad: bfloat16 [16, 6144, 2048], P('dp', 'sp')
- value_weight_grad: float32 [2048, 1024], P('dp')
- gate_weight_grad: float32 [2048, 1024], P('dp')
- mix_weight_grad: float32 [16, 128, 128], replicated
- mix_bias_grad: float32 [16, 128], replicated
- norm_gain_grad: float32 [1024], replicated
- norm_bias_grad: float32 [1024], replicated
All inputs are finite; a program needn't handle non-finite values.
Results may differ from a plain program's by a relative error of at most 0.0054.
Values may be sent and summed in bfloat16 or wider, within the bound.
A program may use at most 128 MiB of HBM per device.

v0:
```python
import jax
import jax.numpy as jnp
from jax import lax
from jax.sharding import PartitionSpec as P

EPSILON = 1e-06


def gelu_slope(values):
    cdf_part = 0.5 * (1.0 + lax.erf(values * 0.7071067811865476))
    pdf_part = jnp.exp(-0.5 * values * values) * 0.3989422804014327
    return cdf_part + values * pdf_part


def mixer_backward(value_act, gate_act, cotangent, norm_gain, norm_bias, mix_weight, mix_bias):
    seq_len, channels = value_act.shape
    groups, block_len = (mix_weight.shape[0], mix_weight.shape[1])
    group_dim = channels // groups
    blocks = seq_len // block_len
    value_float = value_act.astype(jnp.float32)
    gate_float = gate_act.astype(jnp.float32)
    activated = jax.nn.gelu(value_float, approximate=False)
    gate_gelu = jax.nn.gelu(gate_float, approximate=False)
    centred = gate_gelu - jnp.mean(gate_gelu, axis=-1, keepdims=True)
    inv_std = lax.rsqrt(jnp.mean(centred * centred, axis=-1, keepdims=True) + EPSILON)
    normed = centred * inv_std
    spread_in = (normed * norm_gain + norm_bias).astype(jnp.bfloat16)
    spread_in = spread_in.reshape(blocks, block_len, groups, group_dim)
    causal = jnp.tril(jnp.ones((block_len, block_len), dtype=bool))
    masked_weight = jnp.where(causal[None], mix_weight, jnp.zeros_like(mix_weight))
    spatial = jnp.einsum(
        "gts,bsgd->btgd", masked_weight, spread_in, preferred_element_type=jnp.float32
    )
    spatial = (spatial + mix_bias.T[None, :, :, None]).reshape(seq_len, channels)
    grad_out = cotangent.astype(jnp.float32)
    grad_act = grad_out * spatial
    grad_spatial = grad_out * activated
    grad_split = grad_spatial.reshape(blocks, block_len, groups, group_dim)
    bias_grad = jnp.sum(grad_split, axis=(0, 3)).T
    spatial_low = grad_split.astype(jnp.bfloat16)
    weight_grad = jnp.einsum(
        "btgd,bsgd->gts", spatial_low, spread_in, preferred_element_type=jnp.float32
    )
    weight_grad = jnp.where(causal[None], weight_grad, jnp.zeros_like(weight_grad))
    grad_norm = jnp.einsum(
        "gts,btgd->bsgd", masked_weight, spatial_low, preferred_element_type=jnp.float32
    )
    grad_norm = grad_norm.reshape(seq_len, channels)
    gain_grad = jnp.sum(grad_norm * normed, axis=0)
    shift_grad = jnp.sum(grad_norm, axis=0)
    grad_hat = grad_norm * norm_gain
    grad_gate = inv_std * (
        grad_hat
        - jnp.mean(grad_hat, axis=-1, keepdims=True)
        - normed * jnp.mean(grad_hat * normed, axis=-1, keepdims=True)
    )
    value_grad = (grad_act * gelu_slope(value_float)).astype(jnp.bfloat16)
    gate_grad = (grad_gate * gelu_slope(gate_float)).astype(jnp.bfloat16)
    return (value_grad, gate_grad, (weight_grad, bias_grad, gain_grad, shift_grad))


def shards(
    tokens,
    value_act,
    gate_act,
    cotangent,
    value_weight,
    gate_weight,
    norm_gain,
    norm_bias,
    mix_weight,
    mix_bias,
):
    value_grad, gate_grad, stats = mixer_backward(
        value_act[0], gate_act[0], cotangent[0], norm_gain, norm_bias, mix_weight, mix_bias
    )
    channels = value_grad.shape[1]
    both_grads = jnp.concatenate((value_grad, gate_grad), axis=1)
    both_weights = jnp.concatenate((value_weight, gate_weight), axis=1)
    input_grad = lax.dot_general(
        both_grads,
        lax.all_gather(both_weights, "dp", axis=0, tiled=True),
        (((1,), (1,)), ((), ())),
        preferred_element_type=jnp.float32,
    ).astype(jnp.bfloat16)
    inputs = tokens[0]
    shard_terms = lax.psum_scatter(
        lax.dot_general(
            inputs, both_grads, (((0,), (0,)), ((), ())), preferred_element_type=jnp.float32
        ),
        "dp",
        scatter_dimension=0,
        tiled=True,
    )
    weight_sums = lax.psum(shard_terms, "sp")
    totals = lax.psum((stats[0], stats[1], stats[2], stats[3]), ("sp", "dp"))
    return (
        input_grad[None],
        weight_sums[:, :channels],
        weight_sums[:, channels:],
        totals[0],
        totals[1],
        totals[2],
        totals[3],
    )


def solution(mesh):
    placed = (
        P("dp", "sp", None),
        P("dp", "sp", None),
        P("dp", "sp", None),
        P("dp", "sp", None),
        P("dp", None),
        P("dp", None),
        P(),
        P(),
        P(),
        P(),
    )
    return jax.shard_map(
        shards,
        mesh=mesh,
        in_specs=placed,
        out_specs=(P("dp", "sp", None), P("dp", None), P("dp", None), P(), P(), P(), P()),
        check_vma=False,
    )
```

profile of v0, /device:TPU:1, one launch (start us, length us, event | category | flops | bytes accessed | tf_op | source)
XLA Modules:
  0.0 602.4 jit_solution(7592910926025882119)
XLA Ops:
  7.2 0.0 reduce-scatter.2.cloned.1.call-start
  7.2 2.4 copy.20
  9.6 4.5 fusion.96
  14.2 1.9 convert_multiply_fusion.1
  16.1 0.1 mul.187
  16.1 0.1 add.58
  16.2 2.3 copy.28
  18.5 2.3 copy.19
  20.9 0.2 multiply_reduce_fusion.2
  21.1 3.4 reshape.153
  24.6 3.0 convert_multiply_fusion
  27.6 3.6 mul.200
  31.1 3.6 mul.202
  34.7 3.6 mul.177
  38.3 3.6 mul.179
  41.9 5.6 fusion.93
  47.6 4.0 multiply_reduce_fusion
  51.7 1.1 copy-done.5
  52.8 0.5 bitcast_add_fusion
  53.3 1.1 copy.27
  54.5 0.2 copy-done.4
  54.7 0.8 fusion.78
  55.5 1.1 copy.36
  56.6 0.3 copy-done.2
  56.9 1.5 fusion.79
  58.5 0.9 copy-done.8
  59.4 9.4 %convolution_bitcast_fusion = f32[2048,2048]{0,1:T(8,128)} fusion(bf16[1,384,2048]{2,1,0:T(8,128)(2,1)S(1)} %copy-done, bf16[384,1024]{0,1:T(8,128)(2,1)S(1)} %fusion.79, bf16[384,1024]{0,1:T(8,128)(2,1)S(1)} %fusion.78), kind=kOutput, calls=%fused_computation | convolution fusion | flops 3224371200 | bytes 19922944 | tf_op jit(solution)/shard_map/dot_general | solution.py:88
  68.7 0.0 reduce-scatter.2.cloned.1.call-update
  68.8 0.0 all-gather.2.cloned.1.call-start
  68.8 0.9 copy-done.13
  69.7 1.8 pad_maximum_fusion.3
  71.4 0.0 all-gather.2.cloned.1.call-update
  71.5 0.0 all-reduce.4.cloned.1.call-start
  71.5 100.7 %reduce-scatter.2.cloned.1.call-done = f32[128,2048]{0,1:T(8,128)} async-done(((f32[2048,2048]{0,1:T(8,128)}), f32[128,2048]{0,1:T(8,128)}) %reduce-scatter.2.cloned.1.call-update) | async-done | bytes 1048592 | tf_op jit(solution)/shard_map/reduce_scatter | solution.py:87
  172.2 0.0 all-reduce.4.cloned.1.call-update
  172.2 0.3 all-reduce.6.cloned.1.call-start
  172.5 2.9 fusion.80
  175.4 0.0 all-reduce.6.cloned.1.call-update
  175.4 0.1 reduce_sum.73
  175.5 0.1 reduce_sum.75
  175.5 80.6 %all-reduce = (f32[16,128]{1,0:T(8,128)}, f32[1024]{0:T(1024)}, f32[1024]{0:T(1024)}) all-reduce(f32[16,128]{1,0:T(8,128)S(1)} %bitcast.235, f32[1024]{0:T(1024)S(1)} %reduce_sum.73, f32[1024]{0:T(1024)S(1)} %reduce_sum.75), channel_id=1, replica_groups=mesh['sp'=16,'dp'=16] {'sp','dp'}, use_global_device_ids=true, to_apply=%region_8.9 | all-reduce | flops 4096 | bytes 32768 | tf_op jit(solution)/shard_map/psum | solution.py:96
  256.2 8.5 %fusion = bf16[1,384,2048]{2,1,0:T(8,128)(2,1)} fusion(bf16[2048,2048]{1,0:T(8,128)(2,1)} %all-gather.2.cloned.1.call-done, bf16[384,1024]{0,1:T(8,128)(2,1)} %copy-done.8, bf16[384,1024]{0,1:T(8,128)(2,1)} %copy-done.7), kind=kOutput, calls=%fused_computation.2 | convolution fusion | flops 3225157632 | bytes 11534336 | tf_op jit(solution)/shard_map/dot_general | solution.py:80
  264.7 64.8 %all-reduce.4.cloned.1.call-done = f32[128,2048]{0,1:T(8,128)} async-done(((f32[128,2048]{0,1:T(8,128)}), f32[128,2048]{0,1:T(8,128)}) %all-reduce.4.cloned.1.call-update) | async-done | bytes 1048592 | tf_op jit(solution)/shard_map/psum | solution.py:95
  329.5 1.3 fusion.98
  330.8 1.0 copy.38
  331.8 1.0 copy.37
  332.8 260.8 %all-reduce.6.cloned.1.call-done = f32[16,128,128]{2,1,0:T(8,128)} async-done(((f32[16,128,128]{2,1,0:T(8,128)}), f32[16,128,128]{2,1,0:T(8,128)}) %all-reduce.6.cloned.1.call-update) | async-done | bytes 1048592 | tf_op jit(solution)/shard_map/psum | solution.py:96
  593.6 2.3 copy.61
  (34 shorter events, 0.1 us)
Async XLA Ops:
  7.2 52.2 %copy-start = (bf16[1,384,2048]{2,1,0:T(8,128)(2,1)S(1)}, bf16[1,384,2048]{2,1,0:T(8,128)(2,1)}, u32[]{:S(2)}) copy-start(bf16[1,384,2048]{2,1,0:T(8,128)(2,1)} %param.10) | copy-start | bytes 4718596
  7.2 165.0 %reduce-scatter.2.cloned.1.call-start = ((), (), s32[]{:S(2)}) async-start(), calls=%async_computation.2 | async-start | bytes 17825792 | tf_op jit(solution)/shard_map/reduce_scatter | solution.py:87
  9.6 4.5 copy-start.1
  14.2 1.9 copy-start.14
  14.2 2.0 copy-start.16
  41.9 5.6 copy-start.10
  41.9 5.6 copy-start.11
  41.9 5.7 copy-start.12
  47.6 4.1 copy-start.9
  47.6 5.2 copy-start.15
  51.6 1.1 copy-start.5
  53.3 1.1 copy-start.3
  53.3 1.4 copy-start.4
  55.5 2.9 copy-start.7
  55.5 1.4 copy-start.2
  58.4 0.9 copy-start.8
  68.7 0.9 copy-start.13
  68.7 103.7 %copy-start.6 = (f32[3,128,16,64]{1,3,0,2:T(8,128)S(1)}, f32[3,128,16,64]{1,3,0,2:T(8,128)}, u32[]{:S(2)}) copy-start(f32[3,128,16,64]{1,3,0,2:T(8,128)} %copy-done.5) | copy-start | bytes 4718596
  68.8 187.4 %all-gather.2.cloned.1.call-start = ((), (), s32[]{:S(2)}) async-start(), calls=%async_computation.1 | async-start | bytes 8912896 | tf_op jit(solution)/shard_map/all_gather | solution.py:82
  71.5 258.1 %all-reduce.4.cloned.1.call-start = ((), (), s32[]{:S(2)}) async-start(), calls=%async_computation.3 | async-start | bytes 2097152 | tf_op jit(solution)/shard_map/psum | solution.py:95
  172.2 421.4 %all-reduce.6.cloned.1.call-start = ((), (), s32[]{:S(2)}) async-start(), calls=%async_computation.4 | async-start | bytes 2097152 | tf_op jit(solution)/shard_map/psum | solution.py:96
Sparse Core Ops, SparseCore 0:
  68.9 103.2 reduce-scatter.1
  174.6 57.4 all-gather.1
  235.3 94.1 all-reduce.3
  335.4 258.1 all-reduce.5
where the time goes:
time: 604 us; the launch traced here: 602 us
  waiting for transfers between devices  426 us (71%)
  blocking collectives  80.6 us (13%)
  local copies, waits for them, and re-layouts  36.4 us (6%)
  matrix products  25.3 us (4%)
  other arithmetic  19.3 us (3%)
  between operations  14 us (2%)
    psum x1, waiting for transfers between devices, shards(): totals = lax.psum((stats[0], stats[1], stats[2], stats[3]), ('sp', 'dp'))  261 us
    reduce_scatter x1, waiting for transfers between devices, shards(): lax.psum_scatter(lax.dot_general(inputs, both_grads, (((0,), (0,)), ((),...  101 us
    psum x1, blocking collectives, shards(): totals = lax.psum((stats[0], stats[1], stats[2], stats[3]), ('sp', 'dp'))  80.6 us
    psum x1, waiting for transfers between devices, shards(): weight_sums = lax.psum(shard_terms, 'sp')  64.8 us
    unnamed x40, local copies, waits for them, and re-layouts  14.9 us
  transfers between devices with their start and end apart: 4, of which 3 were waited for; matrix products, arithmetic and copies ran while one was open for 3% of the time, Pallas kernels for 0%

commit v1 on v0

v1 whole, which is shorter than its diff:
```python
import functools
import jax
import jax.numpy as jnp
from jax import lax
from jax.experimental import pallas as pl
from jax.experimental.pallas import tpu as pltpu
from jax.sharding import PartitionSpec as P

EPSILON = 1e-06
F32, BF16 = jnp.float32, jnp.bfloat16
NT = (((1,), (1,)), ((), ()))
TN = (((0,), (0,)), ((), ()))
NN = (((1,), (0,)), ((), ()))


def dot(a, b, dims=NN):
    return lax.dot_general(a, b, dims, preferred_element_type=F32)


def split3(v):
    hi = v.astype(BF16)
    rest = v - hi.astype(F32)
    mid = rest.astype(BF16)
    low = (rest - mid.astype(F32)).astype(BF16)
    return hi, mid, low


def phi_terms(v):
    cdf = 0.5 * (1.0 + lax.erf(v * 0.7071067811865476))
    pdf = jnp.exp(-0.5 * v * v) * 0.3989422804014327
    return cdf, cdf + v * pdf


def mixer(va, ga, cot, gain, bias, mixw, mixb, grads, wgrad, stats,
          mcat, mtrn, normed, slope, spread, low, cv, gnorm, inv, gsum, bfull, acc_g, acc_b):
    rows = 16
    row = lax.broadcasted_iota(jnp.int32, (128, 128), 0)
    col = lax.broadcasted_iota(jnp.int32, (128, 128), 1)
    keep = row >= col

    def prep(p, _):
        for h in range(2):
            m = jnp.where(keep, mixw[2 * p + h].astype(F32), 0.0)
            mcat[p, :, h * 128:(h + 1) * 128] = m.astype(BF16)
            mtrn[p, :, h * 128:(h + 1) * 128] = m.T.astype(BF16)
        return 0

    lax.fori_loop(0, 8, prep, 0)
    group = lax.broadcasted_iota(jnp.int32, (16, 1024), 0)
    chan = lax.broadcasted_iota(jnp.int32, (16, 1024), 1) // 64
    pick = jnp.where(group == chan, 1.0, 0.0).astype(BF16)
    parts = split3(mixb[...])
    bfull[...] = dot(parts[0], pick, TN) + dot(parts[1], pick, TN) + dot(parts[2], pick, TN)
    gsum[...] = jnp.zeros_like(gsum)
    acc_g[...] = jnp.zeros_like(acc_g)
    acc_b[...] = jnp.zeros_like(acc_b)

    def first(i, _):
        at = pl.ds(pl.multiple_of(i * rows, rows), rows)
        v = va[at, :].astype(F32)
        cdf, slp = phi_terms(v)
        c = cot[at, :].astype(F32)
        gs = c * (v * cdf)
        low[at, :] = gs.astype(BF16)
        cv[at, :] = c * slp
        inb = pl.ds(pl.multiple_of(lax.rem(i, 8) * rows, rows), rows)
        gsum[inb, :] += gs
        return 0

    lax.fori_loop(0, 24, first, 0)

    def second(i, _):
        at = pl.ds(pl.multiple_of(i * rows, rows), rows)
        v = ga[at, :].astype(F32)
        cdf, slp = phi_terms(v)
        slope[at, :] = slp
        g = v * cdf
        cen = g - jnp.mean(g, axis=-1, keepdims=True)
        s = lax.rsqrt(jnp.mean(cen * cen, axis=-1, keepdims=True) + EPSILON)
        n = cen * s
        normed[at, :] = n
        inv[at, :] = jnp.broadcast_to(s, (rows, 128))
        spread[at, :] = (n * gain[...] + bias[...]).astype(BF16)
        return 0

    lax.fori_loop(0, 24, second, 0)

    lane = lax.broadcasted_iota(jnp.int32, (1, 128), 1)
    m0 = jnp.where(lane < 64, 1.0, 0.0).astype(BF16)
    m1 = jnp.where(lane < 64, 0.0, 1.0).astype(BF16)

    def mix(p, _):
        cols = pl.ds(pl.multiple_of(p * 128, 128), 128)
        wg = None
        for b in range(3):
            r = slice(b * 128, (b + 1) * 128)
            s = spread[r, cols]
            l = low[r, cols]
            stack_s = jnp.concatenate((s * m0, s * m1), axis=0)
            stack_l = jnp.concatenate((l * m0, l * m1), axis=0)
            spatial = dot(mcat[p], stack_s) + bfull[:, cols]
            grads[r, cols] = (cv[r, cols] * spatial).astype(BF16)
            gnorm[r, cols] = dot(mtrn[p], stack_l)
            term = dot(stack_l, s, NT)
            wg = term if wg is None else wg + term
        wgrad[2 * p] = jnp.where(keep, wg[:128], 0.0)
        wgrad[2 * p + 1] = jnp.where(keep, wg[128:], 0.0)
        return 0

    lax.fori_loop(0, 8, mix, 0)

    def last(i, _):
        at = pl.ds(pl.multiple_of(i * rows, rows), rows)
        gn = gnorm[at, :]
        n = normed[at, :]
        gnn = gn * n
        acc_g[...] += gnn
        acc_b[...] += gn
        h = gn * gain[...]
        mean_h = jnp.mean(h, axis=-1, keepdims=True)
        mean_hn = jnp.mean(h * n, axis=-1, keepdims=True)
        s = inv[at, 0:1]
        out = s * (h - mean_h - n * mean_hn)
        grads[at, 1024:2048] = (out * slope[at, :]).astype(BF16)
        return 0

    lax.fori_loop(0, 24, last, 0)
    parts = split3(gsum[...])
    stats[0:16, :] = dot(pick, parts[0], NT) + dot(pick, parts[1], NT) + dot(pick, parts[2], NT)
    tot_g = jnp.sum(acc_g[...], axis=0, keepdims=True)
    tot_b = jnp.sum(acc_b[...], axis=0, keepdims=True)
    for k in range(8):
        stats[16 + k:17 + k, :] = tot_g[:, k * 128:(k + 1) * 128]
        stats[24 + k:25 + k, :] = tot_b[:, k * 128:(k + 1) * 128]


MIXER_SCRATCH = (
    pltpu.VMEM((8, 128, 256), BF16),
    pltpu.VMEM((8, 128, 256), BF16),
    pltpu.VMEM((384, 1024), F32),
    pltpu.VMEM((384, 1024), F32),
    pltpu.VMEM((384, 1024), BF16),
    pltpu.VMEM((384, 1024), BF16),
    pltpu.VMEM((384, 1024), F32),
    pltpu.VMEM((384, 1024), F32),
    pltpu.VMEM((384, 128), F32),
    pltpu.VMEM((128, 1024), F32),
    pltpu.VMEM((128, 1024), F32),
    pltpu.VMEM((16, 1024), F32),
    pltpu.VMEM((16, 1024), F32),
)


def mixer_call(va, ga, cot, gain, bias, mixw, mixb):
    vm = pl.BlockSpec(memory_space=pltpu.VMEM)
    return pl.pallas_call(
        mixer,
        out_shape=(
            jax.ShapeDtypeStruct((384, 2048), BF16),
            jax.ShapeDtypeStruct((16, 128, 128), F32),
            jax.ShapeDtypeStruct((32, 128), F32),
        ),
        in_specs=[vm] * 7,
        out_specs=(vm, vm, vm),
        scratch_shapes=list(MIXER_SCRATCH),
        compiler_params=pltpu.CompilerParams(vmem_limit_bytes=60 * 1024 * 1024),
        name="mixer",
    )(va, ga, cot, gain, bias, mixw, mixb)


def reducer(tokens, grads, vw, gw, wgrad, stats,
            tgrad, vout, gout, mixout, statout,
            tokr, gradr, tt, wbuf,
            sfar, sup, sdn, fup, fdn, own1, agg, rlay, rprev, rnext, s1f, s1b, r2, own2, s2b, r3, fin, allf,
            mrecv, mq, mqb, mr1, mq1, mq1b, mr2, my, maz, max_, macc, mpart, mrp,
            stc, stx, sty, stz, st0,
            tok_s, tok_r, grd_s, grd_r, ring_s, ring_r, pair_s, pair_r, one_s, one_r, two_s, two_r,
            thr_s, thr_r, fou_s, fou_r, mix_s, mix_r, sts_s, sts_r):
    sp = lax.axis_index("sp")
    dp = lax.axis_index("dp")
    y, x = sp // 4, lax.rem(sp, 4)
    z, c = dp // 2, lax.rem(dp, 2)
    pc = 1 - c

    def at(nx=None, ny=None, nz=None, nc=None):
        nx = x if nx is None else nx
        ny = y if ny is None else ny
        nz = z if nz is None else nz
        nc = c if nc is None else nc
        return {"sp": ny * 4 + nx, "dp": nz * 2 + nc}

    def along(axis, k):
        if axis == "x":
            return at(nx=lax.rem(x + k, 4))
        if axis == "y":
            return at(ny=lax.rem(y + k, 4))
        return at(nz=lax.rem(z + k, 8))

    def copy(src, dst, ssem, rsem, to):
        return pltpu.make_async_remote_copy(
            src_ref=src, dst_ref=dst, send_sem=ssem, recv_sem=rsem,
            device_id=to, device_id_type=pl.DeviceIdType.MESH)

    def await_recv(dst, ssem, rsem):
        copy(dst, dst, ssem, rsem, at(nc=pc)).wait_recv()

    def await_send(src, ssem, rsem):
        copy(src, src, ssem, rsem, at(nc=pc)).wait_send()

    barrier = pltpu.get_barrier_semaphore()
    pl.semaphore_signal(barrier, inc=1, device_id=at(nc=pc), device_id_type=pl.DeviceIdType.MESH)
    for k in range(1, 8):
        pl.semaphore_signal(barrier, inc=1, device_id=along("z", k), device_id_type=pl.DeviceIdType.MESH)
    for k in range(1, 16):
        pl.semaphore_signal(barrier, inc=1, device_id={"sp": lax.rem(sp + k, 16), "dp": dp},
                            device_id_type=pl.DeviceIdType.MESH)
    pl.semaphore_wait(barrier, 23)

    for k in range(8):
        lanes = pl.ds(pl.multiple_of((2 * k + pc) * 128, 128), 128)
        copy(tokens.at[:, lanes], tokr.at[k], tok_s.at[0], tok_r.at[0], at(nc=pc)).start()
    for h in range(2):
        copy(grads.at[:, pl.ds(h * 1024, 1024)], gradr.at[h], grd_s.at[h], grd_r.at[h], at(nc=pc)).start()
    shard = (vw, gw)

    def chunk(zz, v, cc):
        return wbuf.at[zz, v, cc]

    def hop(direction, v, h):
        if h == 1:
            src = shard[v]
            origin = z
        else:
            origin = lax.rem(z - (h - 1) + 8, 8) if direction == 0 else lax.rem(z + (h - 1), 8)
            src = chunk(origin, v, c)
        i = (direction * 2 + v) * 4 + h - 1
        return copy(src, chunk(origin, v, c), ring_s.at[i], ring_r.at[i], along("z", 1 if direction == 0 else 7))

    def last_hop(direction, v):
        return 4 if direction == v else 3

    for v in range(2):
        for direction in range(2):
            hop(direction, v, 1).start()
    for v in range(2):
        copy(shard[v], chunk(z, v, c), pair_s.at[v], pair_r.at[v], at(nc=pc)).start()
        wbuf[z, v, c] = shard[v][...]
    for k in range(8):
        copy(wgrad.at[2 * k + pc], mrecv.at[k], mix_s.at[0], mix_r.at[0], at(nc=pc)).start()
    copy(stats, stc, sts_s.at[0], sts_r.at[0], at(nc=pc)).start()

    def ring_step(h):
        for v in range(2):
            for direction in range(2):
                if h > last_hop(direction, v):
                    continue
                hop(direction, v, h).wait_recv()
                if h < last_hop(direction, v):
                    hop(direction, v, h + 1).start()
                origin = lax.rem(z - h + 8, 8) if direction == 0 else lax.rem(z + h, 8)
                i = 2 + (direction * 2 + v) * 4 + h - 1
                copy(chunk(origin, v, c), chunk(origin, v, c), pair_s.at[i], pair_r.at[i], at(nc=pc)).start()

    def await_pair(h):
        for v in range(2):
            if h == 0:
                await_recv(chunk(0, v, 0), pair_s.at[v], pair_r.at[v])
                continue
            for direction in range(2):
                if h <= last_hop(direction, v):
                    i = 2 + (direction * 2 + v) * 4 + h - 1
                    await_recv(chunk(0, v, 0), pair_s.at[i], pair_r.at[i])

    def into_tokens(zz):
        wv = wbuf[zz, 0].reshape(256, 1024)
        wg = wbuf[zz, 1].reshape(256, 1024)
        out = dot(grads[:, 0:1024], wv, NT) + dot(grads[:, 1024:2048], wg, NT)
        tgrad[:, pl.ds(pl.multiple_of(zz * 256, 256), 256)] = out.astype(BF16)

    for k in range(8):
        lanes = pl.ds(pl.multiple_of((2 * k + c) * 128, 128), 128)
        tt[k * 128:(k + 1) * 128, 0:384] = tokens[:, lanes].T
    await_recv(tokr, tok_s.at[0], tok_r.at[0])
    for k in range(8):
        tt[k * 128:(k + 1) * 128, 384:768] = tokr[k].T

    def product(h, dest, m):
        lanes = pl.ds(pl.multiple_of(dest * 256, 256), 256)
        wide = pl.ds(pl.multiple_of(h * 1024 + dest * 256, 256), 256)
        rows = pl.ds(pl.multiple_of(m * 256, 256), 256)
        return (dot(tt[rows, 0:384], grads[:, wide]) + dot(tt[rows, 384:768], gradr[h, :, lanes]))

    axes = ("x", "y")
    place = (x, y)
    for h in range(2):
        await_recv(gradr.at[h], grd_s.at[h], grd_r.at[h])
        me = place[h]
        far, up, dn = lax.rem(me + 2, 4), lax.rem(me + 1, 4), lax.rem(me + 3, 4)

        def tile_far(m, _):
            sfar[h, m] = product(h, far, m).astype(BF16)
            return 0

        def tile_up(m, _):
            v = product(h, up, m)
            fup[h, m] = v
            sup[h, m] = v.astype(BF16)
            return 0

        def tile_dn(m, _):
            v = product(h, dn, m)
            fdn[h, m] = v
            sdn[h, m] = v.astype(BF16)
            return 0

        def tile_own(m, _):
            own1[h, m] = product(h, me, m)
            return 0

        o = h * 6
        lax.fori_loop(0, 4, tile_far, 0)
        copy(sfar.at[h, 0:2], rlay.at[h, 0], one_s.at[o], one_r.at[o], along(axes[h], 1)).start()
        copy(sfar.at[h, 2:4], rlay.at[h, 1], one_s.at[o + 1], one_r.at[o + 1], along(axes[h], 3)).start()
        lax.fori_loop(0, 4, tile_up, 0)
        copy(sup.at[h, 2:4], rprev.at[h, 1], one_s.at[o + 2], one_r.at[o + 2], along(axes[h], 1)).start()
        lax.fori_loop(0, 4, tile_dn, 0)
        copy(sdn.at[h, 0:2], rnext.at[h, 0], one_s.at[o + 3], one_r.at[o + 3], along(axes[h], 3)).start()
        lax.fori_loop(0, 4, tile_own, 0)

    await_recv(stc, sts_s.at[0], sts_r.at[0])
    st0[0] = stats[...] + stc[...]
    stx[x] = st0[0]
    for k in range(1, 4):
        copy(st0.at[0], stx.at[x], sts_s.at[1], sts_r.at[1], along("x", k)).start()
    await_recv(mrecv, mix_s.at[0], mix_r.at[0])
    for k in range(8):
        v = wgrad[2 * k + c] + mrecv[k]
        mq[k] = v.reshape(4, 32, 128)
        mqb[k] = v.astype(BF16).reshape(4, 32, 128)
    for k in range(1, 4):
        copy(mqb.at[:, lax.rem(x + k, 4)], mr1.at[k - 1], mix_s.at[1], mix_r.at[1], along("x", k)).start()

    ring_step(1)

    for h in range(2):
        o = h * 6
        await_recv(rlay.at[h, 0], one_s.at[o], one_r.at[o])
        agg[h, 0] = (fup[h, 0:2] + rlay[h, 0].astype(F32)).astype(BF16)
        copy(agg.at[h, 0], rprev.at[h, 0], one_s.at[o + 4], one_r.at[o + 4], along(axes[h], 1)).start()
        await_recv(rlay.at[h, 1], one_s.at[o + 1], one_r.at[o + 1])
        agg[h, 1] = (fdn[h, 2:4] + rlay[h, 1].astype(F32)).astype(BF16)
        copy(agg.at[h, 1], rnext.at[h, 1], one_s.at[o + 5], one_r.at[o + 5], along(axes[h], 3)).start()

    await_recv(stx.at[pl.ds(0, 3)], sts_s.at[1], sts_r.at[1])
    st0[1] = (stx[0] + stx[1]) + (stx[2] + stx[3])
    sty[y] = st0[1]
    for k in range(1, 4):
        copy(st0.at[1], sty.at[y], sts_s.at[2], sts_r.at[2], along("y", k)).start()
    await_recv(mr1, mix_s.at[1], mix_r.at[1])
    v = mq[:, x] + (mr1[0].astype(F32) + mr1[1].astype(F32)) + mr1[2].astype(F32)
    mq1[...] = v
    mq1b[...] = v.astype(BF16)
    for k in range(1, 8):
        copy(mq1b.at[lax.rem(z + k, 8)], mr2.at[k - 1], mix_s.at[2], mix_r.at[2], along("z", k)).start()

    await_pair(0)
    into_tokens(z)
    ring_step(2)

    await_recv(sty.at[pl.ds(0, 3)], sts_s.at[2], sts_r.at[2])
    st0[2] = (sty[0] + sty[1]) + (sty[2] + sty[3])
    stz[z] = st0[2]
    for k in range(1, 8):
        copy(st0.at[2], stz.at[z], sts_s.at[3], sts_r.at[3], along("z", k)).start()
    await_recv(mr2, mix_s.at[2], mix_r.at[2])
    v = mq1[z]
    for k in range(7):
        v = v + mr2[k].astype(F32)
    mpart[...] = v
    my[y] = v
    for k in range(1, 4):
        copy(mpart, my.at[y], mix_s.at[3], mix_r.at[3], along("y", k)).start()

    for h in range(2):
        o = h * 6
        for i, buf in ((2, rprev.at[h, 1]), (4, rprev.at[h, 0]), (3, rnext.at[h, 0]), (5, rnext.at[h, 1])):
            await_recv(buf, one_s.at[o + i], one_r.at[o + i])
        for q in range(4):
            v = own1[h, q] + (rprev[h, q // 2, q % 2].astype(F32) + rnext[h, q // 2, q % 2].astype(F32))
            v = v.reshape(2, 4, 32, 256)
            s1f[h, 2 * q:2 * q + 2] = v
            s1b[h, 2 * q:2 * q + 2] = v.astype(BF16)
        other = place[1 - h]
        for k in range(1, 4):
            copy(s1b.at[h, :, lax.rem(other + k, 4)], r2.at[h, k - 1], two_s.at[h], two_r.at[h],
                 along(axes[1 - h], k)).start()

    await_pair(1)
    into_tokens(lax.rem(z + 1, 8))
    into_tokens(lax.rem(z + 7, 8))
    ring_step(3)

    await_recv(my.at[pl.ds(0, 3)], mix_s.at[3], mix_r.at[3])
    v = ((my[0] + my[1]) + (my[2] + my[3])).astype(BF16)
    macc[...] = v
    maz[z] = v
    for k in range(1, 8):
        copy(macc, maz.at[z], mix_s.at[4], mix_r.at[4], along("z", k)).start()

    for h in range(2):
        await_recv(r2.at[h], two_s.at[h], two_r.at[h])
        v = s1f[h, :, place[1 - h]] + (r2[h, 0].astype(F32) + r2[h, 1].astype(F32)) + r2[h, 2].astype(F32)
        own2[h] = v
        s2b[h] = v.astype(BF16)
        for k in range(1, 8):
            copy(s2b.at[h, lax.rem(z + k, 8)], r3.at[h, k - 1], thr_s.at[h], thr_r.at[h], along("z", k)).start()

    await_pair(2)
    into_tokens(lax.rem(z + 2, 8))
    into_tokens(lax.rem(z + 6, 8))

    await_recv(maz.at[pl.ds(0, 7)], mix_s.at[4], mix_r.at[4])
    max_[x] = maz[...]
    for k in range(1, 4):
        copy(maz, max_.at[x], mix_s.at[5], mix_r.at[5], along("x", k)).start()

    for h in range(2):
        await_recv(r3.at[h], thr_s.at[h], thr_r.at[h])
        v = own2[h, z]
        for k in range(7):
            v = v + r3[h, k].astype(F32)
        fin[h] = v.astype(BF16)
        allf[sp, h] = v.astype(BF16)
    for k in range(1, 16):
        copy(fin, allf.at[sp], fou_s.at[0], fou_r.at[0], {"sp": lax.rem(sp + k, 16), "dp": dp}).start()

    await_pair(3)
    into_tokens(lax.rem(z + 3, 8))
    into_tokens(lax.rem(z + 5, 8))
    await_recv(max_.at[pl.ds(0, 3)], mix_s.at[5], mix_r.at[5])
    copy(max_, mrp, mix_s.at[6], mix_r.at[6], at(nc=pc)).start()

    await_recv(stz.at[pl.ds(0, 7)], sts_s.at[3], sts_r.at[3])
    t = stz[0]
    for k in range(1, 8):
        t = t + stz[k]
    statout[...] = t

    ring_step(4)
    await_recv(mrp, mix_s.at[6], mix_r.at[6])
    for k in range(8):
        mixout[2 * k + c] = max_[:, k].reshape(128, 128).astype(F32)
        mixout[2 * k + pc] = mrp[:, k].reshape(128, 128).astype(F32)
    await_pair(4)
    into_tokens(lax.rem(z + 4, 8))

    await_recv(allf.at[pl.ds(0, 15)], fou_s.at[0], fou_r.at[0])
    for s in range(16):
        a, b = s // 4, s % 4
        vout[a * 32:(a + 1) * 32, b * 256:(b + 1) * 256] = allf[s, 0].astype(F32)
        gout[b * 32:(b + 1) * 32, a * 256:(a + 1) * 256] = allf[s, 1].astype(F32)

    await_send(tokr, tok_s.at[0], tok_r.at[0])
    for h in range(2):
        await_send(gradr.at[h], grd_s.at[h], grd_r.at[h])
        for i in range(6):
            await_send(agg.at[h, 0], one_s.at[h * 6 + i], one_r.at[h * 6 + i])
        await_send(r2.at[h], two_s.at[h], two_r.at[h])
        await_send(r3.at[h], thr_s.at[h], thr_r.at[h])
    await_send(allf.at[pl.ds(0, 15)], fou_s.at[0], fou_r.at[0])
    for i, buf in enumerate((mrecv, mr1, mr2, my.at[pl.ds(0, 3)], maz.at[pl.ds(0, 7)],
                             max_.at[pl.ds(0, 3)], mrp)):
        await_send(buf, mix_s.at[i], mix_r.at[i])
    for i, buf in enumerate((stc, stx.at[pl.ds(0, 3)], sty.at[pl.ds(0, 3)], stz.at[pl.ds(0, 7)])):
        await_send(buf, sts_s.at[i], sts_r.at[i])
    for v in range(2):
        await_send(shard[v], pair_s.at[v], pair_r.at[v])
        for direction in range(2):
            for h in range(1, last_hop(direction, v) + 1):
                i = (direction * 2 + v) * 4 + h - 1
                await_send(shard[v], ring_s.at[i], ring_r.at[i])
                await_send(shard[v], pair_s.at[2 + i], pair_r.at[2 + i])


REDUCER_SCRATCH = (
    pltpu.VMEM((8, 384, 128), BF16),
    pltpu.VMEM((2, 384, 1024), BF16),
    pltpu.VMEM((1024, 768), BF16),
    pltpu.VMEM((8, 2, 2, 128, 1024), BF16),
    pltpu.VMEM((2, 4, 256, 256), BF16),
    pltpu.VMEM((2, 4, 256, 256), BF16),
    pltpu.VMEM((2, 4, 256, 256), BF16),
    pltpu.VMEM((2, 4, 256, 256), F32),
    pltpu.VMEM((2, 4, 256, 256), F32),
    pltpu.VMEM((2, 4, 256, 256), F32),
    pltpu.VMEM((2, 2, 2, 256, 256), BF16),
    pltpu.VMEM((2, 2, 2, 256, 256), BF16),
    pltpu.VMEM((2, 2, 2, 256, 256), BF16),
    pltpu.VMEM((2, 2, 2, 256, 256), BF16),
    pltpu.VMEM((2, 8, 4, 32, 256), F32),
    pltpu.VMEM((2, 8, 4, 32, 256), BF16),
    pltpu.VMEM((2, 3, 8, 32, 256), BF16),
    pltpu.VMEM((2, 8, 32, 256), F32),
    pltpu.VMEM((2, 8, 32, 256), BF16),
    pltpu.VMEM((2, 7, 32, 256), BF16),
    pltpu.VMEM((2, 32, 256), BF16),
    pltpu.VMEM((16, 2, 32, 256), BF16),
    pltpu.VMEM((8, 128, 128), F32),
    pltpu.VMEM((8, 4, 32, 128), F32),
    pltpu.VMEM((8, 4, 32, 128), BF16),
    pltpu.VMEM((3, 8, 32, 128), BF16),
    pltpu.VMEM((8, 32, 128), F32),
    pltpu.VMEM((8, 32, 128), BF16),
    pltpu.VMEM((7, 32, 128), BF16),
    pltpu.VMEM((4, 32, 128), F32),
    pltpu.VMEM((8, 32, 128), BF16),
    pltpu.VMEM((4, 8, 32, 128), BF16),
    pltpu.VMEM((32, 128), BF16),
    pltpu.VMEM((32, 128), F32),
    pltpu.VMEM((4, 8, 32, 128), BF16),
    pltpu.VMEM((32, 128), F32),
    pltpu.VMEM((4, 32, 128), F32),
    pltpu.VMEM((4, 32, 128), F32),
    pltpu.VMEM((8, 32, 128), F32),
    pltpu.VMEM((3, 32, 128), F32),
    pltpu.SemaphoreType.DMA((1,)), pltpu.SemaphoreType.DMA((1,)),
    pltpu.SemaphoreType.DMA((2,)), pltpu.SemaphoreType.DMA((2,)),
    pltpu.SemaphoreType.DMA((16,)), pltpu.SemaphoreType.DMA((16,)),
    pltpu.SemaphoreType.DMA((18,)), pltpu.SemaphoreType.DMA((18,)),
    pltpu.SemaphoreType.DMA((12,)), pltpu.SemaphoreType.DMA((12,)),
    pltpu.SemaphoreType.DMA((2,)), pltpu.SemaphoreType.DMA((2,)),
    pltpu.SemaphoreType.DMA((2,)), pltpu.SemaphoreType.DMA((2,)),
    pltpu.SemaphoreType.DMA((1,)), pltpu.SemaphoreType.DMA((1,)),
    pltpu.SemaphoreType.DMA((7,)), pltpu.SemaphoreType.DMA((7,)),
    pltpu.SemaphoreType.DMA((4,)), pltpu.SemaphoreType.DMA((4,)),
)


def reducer_call(tokens, grads, vw, gw, wgrad, stats):
    vm = pl.BlockSpec(memory_space=pltpu.VMEM)
    return pl.pallas_call(
        reducer,
        out_shape=(
            jax.ShapeDtypeStruct((384, 2048), BF16),
            jax.ShapeDtypeStruct((128, 1024), F32),
            jax.ShapeDtypeStruct((128, 1024), F32),
            jax.ShapeDtypeStruct((16, 128, 128), F32),
            jax.ShapeDtypeStruct((32, 128), F32),
        ),
        in_specs=[vm] * 6,
        out_specs=(vm,) * 5,
        scratch_shapes=list(REDUCER_SCRATCH),
        compiler_params=pltpu.CompilerParams(
            collective_id=0, has_side_effects=True, vmem_limit_bytes=62 * 1024 * 1024),
        name="reducer",
    )(tokens, grads, vw, gw, wgrad, stats)


def shards(tokens, value_act, gate_act, cotangent, value_weight, gate_weight,
           norm_gain, norm_bias, mix_weight, mix_bias):
    grads, wgrad, stats = mixer_call(
        value_act[0], gate_act[0], cotangent[0], norm_gain[None], norm_bias[None], mix_weight, mix_bias)
    tgrad, vout, gout, mixout, statout = reducer_call(
        tokens[0], grads, value_weight, gate_weight, wgrad, stats)
    return (tgrad[None], vout, gout, mixout, statout[0:16],
            statout[16:24].reshape(1024), statout[24:32].reshape(1024))


def solution(mesh):
    rows = P("dp", "sp", None)
    placed = (rows, rows, rows, rows, P("dp", None), P("dp", None), P(), P(), P(), P())
    return jax.shard_map(
        shards, mesh=mesh, in_specs=placed,
        out_specs=(rows, P("dp", None), P("dp", None), P(), P(), P(), P()), check_vma=False)
```

time: 604 us -> 104 us (0.17)
  waiting for transfers between devices: 426 us -> 0 us
  Pallas kernels: 0 us -> 94.8 us
  blocking collectives: 80.6 us -> 0 us
  local copies, waits for them, and re-layouts: 36.4 us -> 7.96 us
  matrix products: 25.3 us -> 0 us
  other arithmetic: 19.3 us -> 0 us
  between operations: 14 us -> 0.65 us
    psum x2 -> x0, waiting for transfers between devices: 326 us -> none  [the longest x1 261 us: shards(): totals = lax.psum((stats[0], stats[1], stats[2], stats[3]), ('sp', 'dp'))]
    reduce_scatter x1 -> x0, waiting for transfers between devices: 101 us -> none  [shards(): lax.psum_scatter(lax.dot_general(inputs, both_grads, (((0,), (0,)), ((),...]
    pallas_call x0 -> x2, Pallas kernels: none -> 94.8 us  [the longest x1 79.2 us: reducer_call(): pl.pallas_call(reducer, out_shape=(jax.ShapeDtypeStruct((384, 2048), BF16...]
    psum x1 -> x0, blocking collectives: 80.6 us -> none  [shards(): totals = lax.psum((stats[0], stats[1], stats[2], stats[3]), ('sp', 'dp'))]
    dot_general x5 -> x0, matrix products: 25.3 us -> none  [the longest x1 9.36 us: shards(): lax.dot_general(inputs, both_grads, (((0,), (0,)), ((), ())), preferred_e...]
    mul x5 -> x0, local copies, waits for them, and re-layouts: 14.4 us -> none  [the longest x2 7.21 us: mixer_backward(): gate_gelu = jax.nn.gelu(gate_float, approximate=False)]
    reduce_sum x3 -> x0, other arithmetic: 10.4 us -> none  [the longest x1 5.61 us: mixer_backward(): bias_grad = jnp.sum(grad_split, axis=(0, 3)).T]
    unnamed x40 -> x10, local copies, waits for them, and re-layouts: 14.9 us -> 5.38 us
  transfers between devices with their start and end apart: 4 -> 0, of which waited for: 3 -> 0; matrix products, arithmetic and copies ran while one was open for 3% -> 0% of each run, Pallas kernels for 0% -> 0%
where the time goes in v1:
time: 104 us; the launch traced here: 103 us
  Pallas kernels  94.8 us (91%)
  local copies, waits for them, and re-layouts  7.96 us (8%)
    pallas_call x1, Pallas kernels, reducer_call(): pl.pallas_call(reducer, out_shape=(jax.ShapeDtypeStruct((384, 2048), BF16...  79.2 us
    pallas_call x1, Pallas kernels, mixer_call(): pl.pallas_call(mixer, out_shape=(jax.ShapeDtypeStruct((384, 2048), BF16),...  15.7 us
    unnamed x10, local copies, waits for them, and re-layouts  5.38 us

profile of v1, /device:TPU:1, one launch (start us, length us, event | category | flops | bytes accessed | tf_op | source)
XLA Modules:
  0.0 103.4 jit_solution(10226434100197854619)
XLA Ops:
  0.6 15.7 %mixer.1 = (bf16[384,2048]{1,0:T(8,128)(2,1)}, f32[16,128,128]{2,1,0:T(8,128)}, f32[32,128]{1,0:T(8,128)}) custom-call(bf16[384,1024]{1,0:T(8,128)(2,1)} %bitcast.13, bf16[384,1024]{1,0:T(8,128)(2,1)} %bitcast.14, bf16[384,1024]{1,0:T(8,128)(2,1)} %bitcast.15, f32[1,1024]{1,0:T(1,128)} %bitcast.16, f32[1,1024]{1,0:T(1,128)} %bitcast.17, ...), custom_call_target="tpu_custom_call" | custom-call | tf_op jit(solution)/shard_map/mixer/pallas_call | solution.py:156
  16.3 79.2 %reducer.1 = (bf16[384,2048]{1,0:T(8,128)(2,1)}, f32[128,1024]{1,0:T(8,128)}, f32[128,1024]{1,0:T(8,128)}, f32[16,128,128]{2,1,0:T(8,128)}, f32[32,128]{1,0:T(8,128)}) custom-call(bf16[384,2048]{1,0:T(8,128)(2,1)} %bitcast.12, bf16[384,2048]{1,0:T(8,128)(2,1)} %get-tuple-element.15.grads, bf16[128,1024]{1,0:T(8,128)(2,1)} %vw.1, bf16[128,1024]{1,0:T(8,128)(2,1)} %gw.1, ...), custom_call_target="tpu_custom_call" | custom-call | tf_op jit(solution)/shard_map/reducer/pallas_call | solution.py:541
  95.5 1.3 %slice.9 = f32[16,128]{1,0:T(8,128)} slice(f32[32,128]{1,0:T(8,128)} %get-tuple-element.22), slice={[0:16], [0:128]} | slice | bytes 16384 | tf_op jit(solution)/shard_map/slice | solution.py:565
  96.8 1.3 %slice_bitcast_fusion = (f32[1024]{0:T(1024)}, f32[1024]{0:T(1024)}) fusion(f32[32,128]{1,0:T(8,128)} %get-tuple-element.22), kind=kLoop, calls=%fused_computation | loop fusion | bytes 16384 | tf_op jit(solution)/shard_map/reshape | solution.py:566
  98.0 0.0 copy-start.2
  98.1 0.0 copy-start.1
  98.1 2.8 %copy.21 = bf16[1,384,2048]{2,1,0:T(8,128)(2,1)} copy(bf16[1,384,2048]{2,1,0:T(8,128)(2,1)} %bitcast.11) | data formatting | bytes 3145728
  100.9 0.0 copy-done.2
  100.9 0.0 copy-start
  100.9 0.8 copy.22
  101.7 0.0 copy-done.1
  101.7 0.8 copy.23
  102.5 0.0 copy-done
  102.5 1.0 copy.24
Async XLA Ops:
  98.0 2.8 %copy-start.2 = (f32[128,1024]{1,0:T(8,128)S(1)}, f32[128,1024]{1,0:T(8,128)}, u32[]{:S(2)}) copy-start(f32[128,1024]{1,0:T(8,128)} %get-tuple-element.33) | copy-start | bytes 1572868
  98.1 3.6 %copy-start.1 = (f32[128,1024]{1,0:T(8,128)S(1)}, f32[128,1024]{1,0:T(8,128)}, u32[]{:S(2)}) copy-start(f32[128,1024]{1,0:T(8,128)} %get-tuple-element.34) | copy-start | bytes 1572868
  100.9 1.6 %copy-start = (f32[16,128,128]{2,1,0:T(8,128)S(1)}, f32[16,128,128]{2,1,0:T(8,128)}, u32[]{:S(2)}) copy-start(f32[16,128,128]{2,1,0:T(8,128)} %get-tuple-element.35) | copy-start | bytes 3145732

commit v2 on v0

v2 whole, which is shorter than its diff:
```python
import functools
import jax
import jax.numpy as jnp
from jax import lax
from jax.experimental import pallas as pl
from jax.experimental.pallas import tpu as pltpu
from jax.sharding import PartitionSpec as P

EPSILON = 1e-06
F32, BF16 = jnp.float32, jnp.bfloat16
NT = (((1,), (1,)), ((), ()))
TN = (((0,), (0,)), ((), ()))
NN = (((1,), (0,)), ((), ()))


TOP = 96
GATE_UNROLL = 4
LAST_UNROLL = 4
PROFILE = False
_open = []


def mark(name):
    if not PROFILE:
        return
    while _open:
        _open.pop().__exit__(None, None, None)
    if name:
        scope = jax.named_scope(name)
        scope.__enter__()
        _open.append(scope)


def dot(a, b, dims=NN):
    return lax.dot_general(a, b, dims, preferred_element_type=F32)


def split3(v):
    hi = v.astype(BF16)
    rest = v - hi.astype(F32)
    mid = rest.astype(BF16)
    low = (rest - mid.astype(F32)).astype(BF16)
    return hi, mid, low


def phi_terms(v):
    cdf = 0.5 * (1.0 + lax.erf(v * 0.7071067811865476))
    pdf = jnp.exp(-0.5 * v * v) * 0.3989422804014327
    return cdf, cdf + v * pdf


def fused(tokens, va_h, ga_h, cot_h, vw, gw, mixw_h, gain_h, bias_h, mixb_h,
          tgrad_h, wout_h, mixo_h, bout_h, nout_h, hout_h,
          tgrad, wout, mixo, bout, nout, hout, gain, bias, mixb,
          va, ga, cot, mixw, tokl, mcat, mtrn, normed, slope, spread, low, cv, gnorm, inv, gsum, bfull, acc_g, acc_b,
          grads, wgrad, stats,
          tokr, tt, wbuf,
          sfar, sup, sdn, fup, fdn, own1, agg, rlay, rprev, rnext, s1f, s1b, r2, own2, s2b, r3, fin, allf,
          mrecv, mq, mqb, mr1, mq1, mq1b, mr2, my, maz, max_, macc, mpart, mrp,
          stc, stx, sty, stz, stg, st0, st1,
          loc, outs, tok_s, tok_r, grd_s, grd_r, ring_s, ring_r, help_s, help_r, pair_s, pair_r, one_s, one_r, two_s, two_r,
          thr_s, thr_r, fou_s, fou_r, mix_s, mix_r, sts_s, sts_r):
    sp = lax.axis_index("sp")
    dp = lax.axis_index("dp")
    y, x = sp // 4, lax.rem(sp, 4)
    z, c = dp // 2, lax.rem(dp, 2)
    pc = 1 - c

    def at(nx=None, ny=None, nz=None, nc=None):
        nx = x if nx is None else nx
        ny = y if ny is None else ny
        nz = z if nz is None else nz
        nc = c if nc is None else nc
        return {"sp": ny * 4 + nx, "dp": nz * 2 + nc}

    def along(axis, k):
        if axis == "x":
            return at(nx=lax.rem(x + k, 4))
        if axis == "y":
            return at(ny=lax.rem(y + k, 4))
        return at(nz=lax.rem(z + k, 8))

    def copy(src, dst, ssem, rsem, to):
        return pltpu.make_async_remote_copy(
            src_ref=src, dst_ref=dst, send_sem=ssem, recv_sem=rsem,
            device_id=to, device_id_type=pl.DeviceIdType.MESH)

    def await_recv(dst, ssem, rsem):
        copy(dst, dst, ssem, rsem, at(nc=pc)).wait_recv()

    def await_send(src, ssem, rsem):
        copy(src, src, ssem, rsem, at(nc=pc)).wait_send()


    mark("barrier")
    barrier = pltpu.get_barrier_semaphore()
    pl.semaphore_signal(barrier, inc=1, device_id=at(nc=pc), device_id_type=pl.DeviceIdType.MESH)
    for k in range(1, 8):
        pl.semaphore_signal(barrier, inc=1, device_id=along("z", k), device_id_type=pl.DeviceIdType.MESH)
    for k in range(1, 16):
        pl.semaphore_signal(barrier, inc=1, device_id={"sp": lax.rem(sp + k, 16), "dp": dp},
                            device_id_type=pl.DeviceIdType.MESH)
    shard = (vw, gw)
    local = [pltpu.make_async_copy(va_h, va, loc.at[0]), pltpu.make_async_copy(cot_h, cot, loc.at[1]),
             pltpu.make_async_copy(ga_h, ga, loc.at[2])]
    for v in range(2):
        local.append(pltpu.make_async_copy(shard[v], wbuf.at[z, v, c], loc.at[3 + v]))
    for k in range(8):
        lanes = pl.ds(pl.multiple_of((2 * k + c) * 128, 128), 128)
        local.append(pltpu.make_async_copy(tokens.at[:, lanes], tokl.at[k], loc.at[5 + k]))
    local.append(pltpu.make_async_copy(mixw_h, mixw, loc.at[13]))
    local.append(pltpu.make_async_copy(gain_h, gain, loc.at[14]))
    local.append(pltpu.make_async_copy(bias_h, bias, loc.at[15]))
    local.append(pltpu.make_async_copy(mixb_h, mixb, loc.at[16]))
    for n in (0, 1, 2, 14, 15, 16, 13, 5, 6, 7, 8, 9, 10, 11, 12, 3, 4):
        local[n].start()

    axes = ("x", "y")
    place = (x, y)

    def top(zz, v, cc):
        return wbuf.at[zz, v, cc, pl.ds(0, TOP)]

    def low_rows(zz, v, cc):
        return wbuf.at[zz, v, cc, pl.ds(TOP, 128 - TOP)]

    def slice_of(zz, v, cc):
        return wbuf.at[zz, v, cc, pl.ds(TOP, 128 - TOP), pl.ds(pl.multiple_of(place[v] * 256, 256), 256)]

    def came_from(direction, h):
        return lax.rem(z - h + 8, 8) if direction == 0 else lax.rem(z + h, 8)

    def last_hop(direction, v):
        return 4 if direction == v else 3

    def number(direction, v, h):
        return (direction * 2 + v) * 4 + h - 1

    def hop(direction, v, h, part):
        origin = came_from(direction, h - 1)
        dst = (top, slice_of)[part](origin, v, c)
        if h > 1:
            src = dst
        elif part == 0:
            src = shard[v].at[pl.ds(0, TOP)]
        else:
            src = shard[v].at[pl.ds(TOP, 128 - TOP), pl.ds(pl.multiple_of(place[v] * 256, 256), 256)]
        i = number(direction, v, h) + 16 * part
        return copy(src, dst, ring_s.at[i], ring_r.at[i], along("z", 1 if direction == 0 else 7))

    def directions(h, v):
        return [d for d in range(2) if h <= last_hop(d, v)]

    def ring_part(h, v, part):
        for d in directions(h, v):
            hop(d, v, h, part).wait_recv()
            if h < last_hop(d, v):
                hop(d, v, h + 1, part).start()

    def ring_step(h, v):
        if h > 1:
            ring_part(h, v, 1)
        ring_part(h, v, 0)
        for d in directions(h, v):
            ref = top(came_from(d, h), v, c)
            i = 2 + number(d, v, h)
            copy(ref, ref, pair_s.at[i], pair_r.at[i], at(nc=pc)).start()

    def help_out(h, v):
        for d in directions(h, v):
            i = number(d, v, h)
            ref = slice_of(came_from(d, h), v, c)
            for k in range(1, 4):
                copy(ref, ref, help_s.at[i], help_r.at[i], along(axes[v], k)).start()

    def helped(d, v, h):
        ref = wbuf.at[0, v, 0, pl.ds(TOP, 128 - TOP), pl.ds(0, 768)]
        return copy(ref, ref, help_s.at[number(d, v, h)], help_r.at[number(d, v, h)], at(nc=pc))

    def help_pair(h):
        for v in range(2):
            for d in directions(h, v):
                helped(d, v, h).wait_recv()
                ref = low_rows(came_from(d, h), v, c)
                i = 18 + number(d, v, h)
                copy(ref, ref, pair_s.at[i], pair_r.at[i], at(nc=pc)).start()

    def await_pair(h):
        for v in range(2):
            if h == 0:
                await_recv(wbuf.at[0, v, 0], pair_s.at[v], pair_r.at[v])
                continue
            for d in directions(h, v):
                i = number(d, v, h)
                await_recv(top(0, v, 0), pair_s.at[2 + i], pair_r.at[2 + i])
                await_recv(low_rows(0, v, 0), pair_s.at[18 + i], pair_r.at[18 + i])

    def into_tokens(zz):
        wv = wbuf[zz, 0].reshape(256, 1024)
        wg = wbuf[zz, 1].reshape(256, 1024)
        out = dot(grads[0:384, 0:1024], wv, NT) + dot(grads[0:384, 1024:2048], wg, NT)
        tgrad[:, pl.ds(pl.multiple_of(zz * 256, 256), 256)] = out.astype(BF16)

    rows = 16
    row = lax.broadcasted_iota(jnp.int32, (128, 128), 0)
    col = lax.broadcasted_iota(jnp.int32, (128, 128), 1)
    keep = row >= col

    gsum[...] = jnp.zeros_like(gsum)
    acc_g[...] = jnp.zeros_like(acc_g)
    acc_b[...] = jnp.zeros_like(acc_b)
    mark("m_value")
    local[0].wait()
    local[1].wait()
    def first(i, _):
        at = pl.ds(pl.multiple_of(i * rows, rows), rows)
        v = va[at, :].astype(F32)
        cdf, slp = phi_terms(v)
        c = cot[at, :].astype(F32)
        gs = c * (v * cdf)
        low[at, :] = gs.astype(BF16)
        cv[at, :] = c * slp
        inb = pl.ds(pl.multiple_of(lax.rem(i, 8) * rows, rows), rows)
        gsum[inb, :] += gs
        return 0

    lax.fori_loop(0, 24, first, 0)

    mark("barrierwait")
    pl.semaphore_wait(barrier, 23)
    for part in (1, 0):
        for v in range(2):
            for direction in range(2):
                hop(direction, v, 1, part).start()
    for k in range(8):
        lanes = pl.ds(pl.multiple_of((2 * k + pc) * 128, 128), 128)
        copy(tokens.at[:, lanes], tokr.at[k], tok_s.at[0], tok_r.at[0], at(nc=pc)).start()
    for v in range(2):
        copy(shard[v], wbuf.at[z, v, c], pair_s.at[v], pair_r.at[v], at(nc=pc)).start()

    mark("m_gate")
    local[2].wait()
    local[14].wait()
    local[15].wait()
    def second(i, _):
        for u in range(GATE_UNROLL):
            rat = pl.ds(pl.multiple_of((i * GATE_UNROLL + u) * rows, rows), rows)
            v = ga[rat, :].astype(F32)
            cdf, slp = phi_terms(v)
            slope[rat, :] = slp
            g = v * cdf
            cen = g - jnp.mean(g, axis=-1, keepdims=True)
            s = lax.rsqrt(jnp.mean(cen * cen, axis=-1, keepdims=True) + EPSILON)
            n = cen * s
            normed[rat, :] = n
            inv[rat, :] = jnp.broadcast_to(s, (rows, 128))
            spread[rat, :] = (n * gain[...] + bias[...]).astype(BF16)
        return 0

    lax.fori_loop(0, 24 // GATE_UNROLL, second, 0)

    mark("m_prep")
    local[13].wait()
    def prep(p, _):
        for h in range(2):
            m = jnp.where(keep, mixw[2 * p + h].astype(F32), 0.0)
            mcat[p, :, h * 128:(h + 1) * 128] = m.astype(BF16)
            mtrn[p, :, h * 128:(h + 1) * 128] = m.T.astype(BF16)
        return 0

    lax.fori_loop(0, 8, prep, 0)
    group = lax.broadcasted_iota(jnp.int32, (16, 1024), 0)
    chan = lax.broadcasted_iota(jnp.int32, (16, 1024), 1) // 64
    pick = jnp.where(group == chan, 1.0, 0.0).astype(BF16)
    local[16].wait()
    parts = split3(mixb[...])
    bfull[...] = dot(parts[0], pick, TN) + dot(parts[1], pick, TN) + dot(parts[2], pick, TN)

    mark("transpose")
    for k in range(8):
        local[5 + k].wait()
        tt[k * 128:(k + 1) * 128, 0:384] = tokl[k].T
    await_recv(tokr, tok_s.at[0], tok_r.at[0])
    for k in range(8):
        tt[k * 128:(k + 1) * 128, 384:768] = tokr[k].T
    mark("help1")
    for v in range(2):
        ring_part(1, v, 1)
        help_out(1, v)
    mark("m_mix")
    lane = lax.broadcasted_iota(jnp.int32, (1, 128), 1)
    m0 = jnp.where(lane < 64, 1.0, 0.0).astype(BF16)
    m1 = jnp.where(lane < 64, 0.0, 1.0).astype(BF16)

    def mix(p, _):
        cols = pl.ds(pl.multiple_of(p * 128, 128), 128)
        wg = None
        for b in range(3):
            r = slice(b * 128, (b + 1) * 128)
            s = spread[r, cols]
            l = low[r, cols]
            stack_s = jnp.concatenate((s * m0, s * m1), axis=0)
            stack_l = jnp.concatenate((l * m0, l * m1), axis=0)
            spatial = dot(mcat[p], stack_s) + bfull[:, cols]
            grads[r, cols] = (cv[r, cols] * spatial).astype(BF16)
            gnorm[r, cols] = dot(mtrn[p], stack_l)
            term = dot(stack_l, s, NT)
            wg = term if wg is None else wg + term
        wgrad[2 * p] = jnp.where(keep, wg[:128], 0.0)
        wgrad[2 * p + 1] = jnp.where(keep, wg[128:], 0.0)
        return 0

    lax.fori_loop(0, 8, mix, 0)

    def swap(h):
        lanes = pl.ds(h * 1024, 1024)
        return copy(grads.at[pl.ds(0, 384), lanes], grads.at[pl.ds(384, 384), lanes], grd_s.at[h], grd_r.at[h], at(nc=pc))

    swap(0).start()
    for k in range(8):
        copy(wgrad.at[2 * k + pc], mrecv.at[k], mix_s.at[0], mix_r.at[0], at(nc=pc)).start()

    mark("m_last")
    def last(i, _):
        for u in range(LAST_UNROLL):
            rat = pl.ds(pl.multiple_of((i * LAST_UNROLL + u) * rows, rows), rows)
            gn = gnorm[rat, :]
            n = normed[rat, :]
            gnn = gn * n
            acc_g[...] += gnn
            acc_b[...] += gn
            h = gn * gain[...]
            mean_h = jnp.mean(h, axis=-1, keepdims=True)
            mean_hn = jnp.mean(h * n, axis=-1, keepdims=True)
            s = inv[rat, 0:1]
            out = s * (h - mean_h - n * mean_hn)
            grads[rat, 1024:2048] = (out * slope[rat, :]).astype(BF16)
        return 0

    lax.fori_loop(0, 24 // LAST_UNROLL, last, 0)
    swap(1).start()
    mark("m_stats")
    parts = split3(gsum[...])
    stats[0:16, :] = dot(pick, parts[0], NT) + dot(pick, parts[1], NT) + dot(pick, parts[2], NT)
    tot_g = jnp.sum(acc_g[...], axis=0, keepdims=True)
    tot_b = jnp.sum(acc_b[...], axis=0, keepdims=True)
    for k in range(8):
        stats[16 + k:17 + k, :] = tot_g[:, k * 128:(k + 1) * 128]
        stats[24 + k:25 + k, :] = tot_b[:, k * 128:(k + 1) * 128]
    copy(stats, stc, sts_s.at[0], sts_r.at[0], at(nc=pc)).start()
    def product(h, dest, half):
        wide = pl.ds(pl.multiple_of(h * 1024 + dest * 256, 256), 256)
        return dot(tt[half * 512:(half + 1) * 512, :], grads[:, wide]).reshape(2, 256, 256)

    def one(i, h, src, dst, k):
        return copy(src, dst, one_s.at[h * 6 + i], one_r.at[h * 6 + i], along(axes[h], k))

    def far_tiles(h):
        mark(f"far{h}")
        dest = lax.rem(place[h] + 2, 4)
        sfar[h, 0:2] = product(h, dest, 0).astype(BF16)
        one(0, h, sfar.at[h, 0:2], rlay.at[h, 0], 1).start()
        sfar[h, 2:4] = product(h, dest, 1).astype(BF16)
        one(1, h, sfar.at[h, 2:4], rlay.at[h, 1], 3).start()

    def near_tiles(h):
        mark(f"near{h}")
        up, dn = lax.rem(place[h] + 1, 4), lax.rem(place[h] + 3, 4)
        sup[h, 2:4] = product(h, up, 1).astype(BF16)
        one(2, h, sup.at[h, 2:4], rprev.at[h, 1], 1).start()
        sdn[h, 0:2] = product(h, dn, 0).astype(BF16)
        one(3, h, sdn.at[h, 0:2], rnext.at[h, 0], 3).start()
        fup[h, 0:2] = product(h, up, 0)
        fdn[h, 2:4] = product(h, dn, 1)

    def own_tiles(h):
        mark(f"own{h}")
        own1[h, 0:2] = product(h, place[h], 0)
        own1[h, 2:4] = product(h, place[h], 1)

    def relay(h):
        mark(f"relay{h}")
        one(0, h, rlay.at[h, 0], rlay.at[h, 0], 1).wait_recv()
        agg[h, 0] = (fup[h, 0:2] + rlay[h, 0].astype(F32)).astype(BF16)
        one(4, h, agg.at[h, 0], rprev.at[h, 0], 1).start()
        one(1, h, rlay.at[h, 1], rlay.at[h, 1], 3).wait_recv()
        agg[h, 1] = (fdn[h, 2:4] + rlay[h, 1].astype(F32)).astype(BF16)
        one(5, h, agg.at[h, 1], rnext.at[h, 1], 3).start()

    def stats_x():
        mark("stats_x")
        await_recv(stc, sts_s.at[0], sts_r.at[0])
        st0[...] = (stats[...] + stc[...]).reshape(4, 8, 128)
        for k in range(1, 4):
            copy(st0.at[lax.rem(x + k, 4)], stx.at[k - 1], sts_s.at[1], sts_r.at[1], along("x", k)).start()

    def stats_y():
        mark("stats_y")
        await_recv(stx, sts_s.at[1], sts_r.at[1])
        st1[0] = ((st0[x] + stx[0]) + stx[1]) + stx[2]
        sty[y] = st1[0]
        for k in range(1, 4):
            copy(st1.at[0], sty.at[y], sts_s.at[2], sts_r.at[2], along("y", k)).start()

    def stats_z():
        mark("stats_z")
        await_recv(sty.at[pl.ds(0, 3)], sts_s.at[2], sts_r.at[2])
        st1[1] = (sty[0] + sty[1]) + (sty[2] + sty[3])
        stz[z] = st1[1]
        for k in range(1, 8):
            copy(st1.at[1], stz.at[z], sts_s.at[3], sts_r.at[3], along("z", k)).start()

    def stats_back():
        mark("stats_back")
        await_recv(stz.at[pl.ds(0, 7)], sts_s.at[3], sts_r.at[3])
        t = stz[0]
        for k in range(1, 8):
            t = t + stz[k]
        st1[2] = t
        stg[x] = t
        for k in range(1, 4):
            copy(st1.at[2], stg.at[x], sts_s.at[4], sts_r.at[4], along("x", k)).start()

    def stats_end():
        mark("stats_end")
        await_recv(stg.at[pl.ds(0, 3)], sts_s.at[4], sts_r.at[4])
        bout[0:8] = stg[0]
        bout[8:16] = stg[1]
        nout[...] = stg[2]
        hout[...] = stg[3]
        for n in (3, 4, 5):
            put[n].start()

    def mix_z():
        mark("mix_z")
        await_recv(mrecv, mix_s.at[0], mix_r.at[0])
        for k in range(8):
            v = wgrad[2 * k + c] + mrecv[k]
            mq[k] = v
            mqb[k] = v.astype(BF16)
        for k in range(1, 8):
            copy(mqb.at[lax.rem(z + k, 8)], mr2.at[k - 1], mix_s.at[1], mix_r.at[1], along("z", k)).start()

    def mix_x():
        mark("mix_x")
        await_recv(mr2, mix_s.at[1], mix_r.at[1])
        v = mq[z]
        for k in range(7):
            v = v + mr2[k].astype(F32)
        v = v.reshape(4, 32, 128)
        mq1[...] = v
        mq1b[...] = v.astype(BF16)
        for k in range(1, 4):
            copy(mq1b.at[lax.rem(x + k, 4)], mr1.at[k - 1], mix_s.at[2], mix_r.at[2], along("x", k)).start()

    def mix_y():
        mark("mix_y")
        await_recv(mr1, mix_s.at[2], mix_r.at[2])
        v = mq1[x] + (mr1[0].astype(F32) + mr1[1].astype(F32)) + mr1[2].astype(F32)
        mpart[...] = v
        my[y] = v
        for k in range(1, 4):
            copy(mpart, my.at[y], mix_s.at[3], mix_r.at[3], along("y", k)).start()

    def mix_back_z():
        mark("mix_back_z")
        await_recv(my.at[pl.ds(0, 3)], mix_s.at[3], mix_r.at[3])
        v = ((my[0] + my[1]) + (my[2] + my[3])).astype(BF16)
        macc[...] = v
        maz[z] = v
        for k in range(1, 8):
            copy(macc, maz.at[z], mix_s.at[4], mix_r.at[4], along("z", k)).start()

    def mix_back_x():
        mark("mix_back_x")
        await_recv(maz.at[pl.ds(0, 7)], mix_s.at[4], mix_r.at[4])
        max_[x] = maz[...]
        for k in range(1, 4):
            copy(maz, max_.at[x], mix_s.at[5], mix_r.at[5], along("x", k)).start()

    def mix_back_c():
        mark("mix_back_c")
        await_recv(max_.at[pl.ds(0, 3)], mix_s.at[5], mix_r.at[5])
        copy(max_, mrp, mix_s.at[6], mix_r.at[6], at(nc=pc)).start()

    def mix_end():
        mark("mix_end")
        await_recv(mrp, mix_s.at[6], mix_r.at[6])
        for k in range(8):
            mixo[2 * k + c] = max_[:, k].reshape(128, 128)
            mixo[2 * k + pc] = mrp[:, k].reshape(128, 128)
        put[2].start()

    def ring(h, v):
        mark(f"ring{h}{v}")
        ring_step(h, v)

    def into(h):
        mark(f"into{h}")
        await_pair(h)
        if h == 0:
            local[3].wait()
            local[4].wait()
            into_tokens(z)
            return
        into_tokens(lax.rem(z + h, 8))
        if h < 4:
            into_tokens(lax.rem(z + 8 - h, 8))

    put = [pltpu.make_async_copy(tgrad, tgrad_h, outs.at[0]), pltpu.make_async_copy(wout.at[0], wout_h.at[0], outs.at[1]),
           pltpu.make_async_copy(mixo, mixo_h, outs.at[2]), pltpu.make_async_copy(bout, bout_h, outs.at[3]),
           pltpu.make_async_copy(nout, nout_h, outs.at[4]), pltpu.make_async_copy(hout, hout_h, outs.at[5]),
           pltpu.make_async_copy(wout.at[1], wout_h.at[1], outs.at[6])]

    def stage_two(h):
        mark(f"two{h}")
        for i, buf in ((2, rprev.at[h, 1]), (4, rprev.at[h, 0]), (3, rnext.at[h, 0]), (5, rnext.at[h, 1])):
            one(i, h, buf, buf, 1).wait_recv()
        for q in range(4):
            v = own1[h, q] + (rprev[h, q // 2, q % 2].astype(F32) + rnext[h, q // 2, q % 2].astype(F32))
            v = v.reshape(2, 4, 32, 256)
            s1f[h, 2 * q:2 * q + 2] = v
            s1b[h, 2 * q:2 * q + 2] = v.astype(BF16)
        other = place[1 - h]
        for k in range(1, 4):
            copy(s1b.at[h, :, lax.rem(other + k, 4)], r2.at[h, k - 1], two_s.at[h], two_r.at[h],
                 along(axes[1 - h], k)).start()

    def stage_three(h):
        mark(f"three{h}")
        await_recv(r2.at[h], two_s.at[h], two_r.at[h])
        v = s1f[h, :, place[1 - h]] + (r2[h, 0].astype(F32) + r2[h, 1].astype(F32)) + r2[h, 2].astype(F32)
        own2[h] = v
        s2b[h] = v.astype(BF16)
        for k in range(1, 8):
            copy(s2b.at[h, lax.rem(z + k, 8)], r3.at[h, k - 1], thr_s.at[h], thr_r.at[h], along("z", k)).start()

    def stage_four(h):
        mark(f"four{h}")
        await_recv(r3.at[h], thr_s.at[h], thr_r.at[h])
        v = own2[h, z]
        for k in range(7):
            v = v + r3[h, k].astype(F32)
        fin[h] = v.astype(BF16)
        allf[h, sp] = v.astype(BF16)
        for k in range(1, 16):
            copy(fin.at[h], allf.at[h, sp], fou_s.at[h], fou_r.at[h], {"sp": lax.rem(sp + k, 16), "dp": dp}).start()

    def stage_end(h):
        mark(f"end{h}")
        await_recv(allf.at[h, pl.ds(0, 15)], fou_s.at[h], fou_r.at[h])
        for s in range(16):
            a, b = (s // 4, s % 4) if h == 0 else (s % 4, s // 4)
            wout[h, a * 32:(a + 1) * 32, b * 256:(b + 1) * 256] = allf[h, s]
        put[(1, 6)[h]].start()

    swap(0).wait_recv()
    far_tiles(0)
    ring(1, 0)
    swap(1).wait_recv()
    far_tiles(1)
    mix_z()
    ring(1, 1)
    near_tiles(0)
    near_tiles(1)
    stats_x()
    own_tiles(0)
    own_tiles(1)
    relay(0)
    relay(1)
    ring(2, 0)
    into(0)
    ring(2, 1)
    help_pair(1)
    into(1)
    ring(3, 0)
    stage_two(0)
    stage_two(1)
    stats_y()
    mix_x()
    for v in range(2):
        help_out(2, v)
    ring(3, 1)
    stage_three(0)
    stage_three(1)
    mix_y()
    stats_z()
    for v in range(2):
        help_out(3, v)
    mark("help_pair2")
    help_pair(2)
    into(2)
    ring(4, 0)
    ring(4, 1)
    for v in range(2):
        help_out(4, v)
    mix_back_z()
    stage_four(0)
    stage_four(1)
    mark("help_pair3")
    help_pair(3)
    into(3)
    mix_back_x()
    stats_back()
    mark("help_pair4")
    help_pair(4)
    into(4)
    put[0].start()
    mix_back_c()
    stats_end()
    mix_end()
    stage_end(0)
    stage_end(1)

    mark("sends")
    for one_out in put:
        one_out.wait()
    await_send(tokr, tok_s.at[0], tok_r.at[0])
    for h in range(2):
        swap(h).wait_send()
        for i in range(6):
            await_send(agg.at[h, 0], one_s.at[h * 6 + i], one_r.at[h * 6 + i])
        await_send(r2.at[h], two_s.at[h], two_r.at[h])
        await_send(r3.at[h], thr_s.at[h], thr_r.at[h])
        await_send(allf.at[h, pl.ds(0, 15)], fou_s.at[h], fou_r.at[h])
    for i, buf in enumerate((mrecv, mr2, mr1, my.at[pl.ds(0, 3)], maz.at[pl.ds(0, 7)],
                             max_.at[pl.ds(0, 3)], mrp)):
        await_send(buf, mix_s.at[i], mix_r.at[i])
    for i, buf in enumerate((stc, stx, sty.at[pl.ds(0, 3)], stz.at[pl.ds(0, 7)], stg.at[pl.ds(0, 3)])):
        await_send(buf, sts_s.at[i], sts_r.at[i])
    for v in range(2):
        await_send(shard[v], pair_s.at[v], pair_r.at[v])
        for h in range(1, 5):
            for d in directions(h, v):
                i = number(d, v, h)
                hop(d, v, h, 0).wait_send()
                hop(d, v, h, 1).wait_send()
                helped(d, v, h).wait_send()
                await_send(top(0, v, 0), pair_s.at[2 + i], pair_r.at[2 + i])
                await_send(low_rows(0, v, 0), pair_s.at[18 + i], pair_r.at[18 + i])
    mark(None)


SCRATCH = (
    pltpu.VMEM((384, 2048), BF16),
    pltpu.VMEM((2, 128, 1024), BF16),
    pltpu.VMEM((16, 128, 128), BF16),
    pltpu.VMEM((16, 128), F32),
    pltpu.VMEM((8, 128), F32),
    pltpu.VMEM((8, 128), F32),
    pltpu.VMEM((1, 1024), F32),
    pltpu.VMEM((1, 1024), F32),
    pltpu.VMEM((16, 128), F32),
    pltpu.VMEM((384, 1024), BF16),
    pltpu.VMEM((384, 1024), BF16),
    pltpu.VMEM((384, 1024), BF16),
    pltpu.VMEM((16, 128, 128), BF16),
    pltpu.VMEM((8, 384, 128), BF16),
    pltpu.VMEM((8, 128, 256), BF16),
    pltpu.VMEM((8, 128, 256), BF16),
    pltpu.VMEM((384, 1024), F32),
    pltpu.VMEM((384, 1024), F32),
    pltpu.VMEM((384, 1024), BF16),
    pltpu.VMEM((384, 1024), BF16),
    pltpu.VMEM((384, 1024), F32),
    pltpu.VMEM((384, 1024), F32),
    pltpu.VMEM((384, 128), F32),
    pltpu.VMEM((128, 1024), F32),
    pltpu.VMEM((128, 1024), F32),
    pltpu.VMEM((16, 1024), F32),
    pltpu.VMEM((16, 1024), F32),
    pltpu.VMEM((768, 2048), BF16),
    pltpu.VMEM((16, 128, 128), F32),
    pltpu.VMEM((32, 128), F32),
    pltpu.VMEM((8, 384, 128), BF16),
    pltpu.VMEM((1024, 768), BF16),
    pltpu.VMEM((8, 2, 2, 128, 1024), BF16),
    pltpu.VMEM((2, 4, 256, 256), BF16),
    pltpu.VMEM((2, 4, 256, 256), BF16),
    pltpu.VMEM((2, 4, 256, 256), BF16),
    pltpu.VMEM((2, 4, 256, 256), F32),
    pltpu.VMEM((2, 4, 256, 256), F32),
    pltpu.VMEM((2, 4, 256, 256), F32),
    pltpu.VMEM((2, 2, 2, 256, 256), BF16),
    pltpu.VMEM((2, 2, 2, 256, 256), BF16),
    pltpu.VMEM((2, 2, 2, 256, 256), BF16),
    pltpu.VMEM((2, 2, 2, 256, 256), BF16),
    pltpu.VMEM((2, 8, 4, 32, 256), F32),
    pltpu.VMEM((2, 8, 4, 32, 256), BF16),
    pltpu.VMEM((2, 3, 8, 32, 256), BF16),
    pltpu.VMEM((2, 8, 32, 256), F32),
    pltpu.VMEM((2, 8, 32, 256), BF16),
    pltpu.VMEM((2, 7, 32, 256), BF16),
    pltpu.VMEM((2, 32, 256), BF16),
    pltpu.VMEM((2, 16, 32, 256), BF16),
    pltpu.VMEM((8, 128, 128), F32),
    pltpu.VMEM((8, 128, 128), F32),
    pltpu.VMEM((8, 128, 128), BF16),
    pltpu.VMEM((3, 32, 128), BF16),
    pltpu.VMEM((4, 32, 128), F32),
    pltpu.VMEM((4, 32, 128), BF16),
    pltpu.VMEM((7, 128, 128), BF16),
    pltpu.VMEM((4, 32, 128), F32),
    pltpu.VMEM((8, 32, 128), BF16),
    pltpu.VMEM((4, 8, 32, 128), BF16),
    pltpu.VMEM((32, 128), BF16),
    pltpu.VMEM((32, 128), F32),
    pltpu.VMEM((4, 8, 32, 128), BF16),
    pltpu.VMEM((32, 128), F32),
    pltpu.VMEM((3, 8, 128), F32),
    pltpu.VMEM((4, 8, 128), F32),
    pltpu.VMEM((8, 8, 128), F32),
    pltpu.VMEM((4, 8, 128), F32),
    pltpu.VMEM((4, 8, 128), F32),
    pltpu.VMEM((3, 8, 128), F32),
    pltpu.SemaphoreType.DMA((17,)), pltpu.SemaphoreType.DMA((7,)),
    pltpu.SemaphoreType.DMA((1,)), pltpu.SemaphoreType.DMA((1,)),
    pltpu.SemaphoreType.DMA((2,)), pltpu.SemaphoreType.DMA((2,)),
    pltpu.SemaphoreType.DMA((32,)), pltpu.SemaphoreType.DMA((32,)),
    pltpu.SemaphoreType.DMA((16,)), pltpu.SemaphoreType.DMA((16,)),
    pltpu.SemaphoreType.DMA((34,)), pltpu.SemaphoreType.DMA((34,)),
    pltpu.SemaphoreType.DMA((12,)), pltpu.SemaphoreType.DMA((12,)),
    pltpu.SemaphoreType.DMA((2,)), pltpu.SemaphoreType.DMA((2,)),
    pltpu.SemaphoreType.DMA((2,)), pltpu.SemaphoreType.DMA((2,)),
    pltpu.SemaphoreType.DMA((2,)), pltpu.SemaphoreType.DMA((2,)),
    pltpu.SemaphoreType.DMA((7,)), pltpu.SemaphoreType.DMA((7,)),
    pltpu.SemaphoreType.DMA((5,)), pltpu.SemaphoreType.DMA((5,)),
)


def fused_call(tokens, va, ga, cot, vw, gw, mixw, gain, bias, mixb):
    hbm = pl.BlockSpec(memory_space=pl.ANY)
    return pl.pallas_call(
        fused,
        out_shape=(
            jax.ShapeDtypeStruct((384, 2048), BF16),
            jax.ShapeDtypeStruct((2, 128, 1024), BF16),
            jax.ShapeDtypeStruct((16, 128, 128), BF16),
            jax.ShapeDtypeStruct((16, 128), F32),
            jax.ShapeDtypeStruct((8, 128), F32),
            jax.ShapeDtypeStruct((8, 128), F32),
        ),
        in_specs=[hbm] * 10,
        out_specs=(hbm,) * 6,
        scratch_shapes=list(SCRATCH),
        compiler_params=pltpu.CompilerParams(
            collective_id=0, has_side_effects=True, vmem_limit_bytes=62 * 1024 * 1024),
        name="fused",
    )(tokens, va, ga, cot, vw, gw, mixw, gain, bias, mixb)


def finish(tgrad, wsum, mixs, bsum, nsum, hsum, tout, vout, gout, mout, bout, nout, hout,
           tbuf, wbuf, wide, mbuf, mwide, bbuf, nbuf, hbuf, isem, osem):
    small = ((bsum, bbuf, bout), (nsum, nbuf, nout), (hsum, hbuf, hout))
    gets = [pltpu.make_async_copy(wsum.at[0], wbuf.at[0], isem.at[0]), pltpu.make_async_copy(wsum.at[1], wbuf.at[1], isem.at[1]),
            pltpu.make_async_copy(mixs, mbuf, isem.at[2])]
    puts = [pltpu.make_async_copy(wide.at[0], vout, osem.at[0]), pltpu.make_async_copy(wide.at[1], gout, osem.at[1]),
            pltpu.make_async_copy(mwide, mout, osem.at[2])]
    for k, (src, buf, dst) in enumerate(small):
        gets.append(pltpu.make_async_copy(src, buf, isem.at[3 + k]))
        puts.append(pltpu.make_async_copy(buf, dst, osem.at[3 + k]))
    for k in range(4):
        rows = pl.ds(k * 96, 96)
        gets.append(pltpu.make_async_copy(tgrad.at[rows], tbuf.at[rows], isem.at[6 + k]))
        puts.append(pltpu.make_async_copy(tbuf.at[rows], tout.at[rows], osem.at[6 + k]))
    for get in gets:
        get.start()
    for k in range(2):
        gets[k].wait()
        wide[k] = wbuf[k].astype(F32)
        puts[k].start()
    gets[2].wait()
    mwide[...] = mbuf[...].astype(F32)
    puts[2].start()
    for k in range(3, 10):
        gets[k].wait()
        puts[k].start()
    for put in puts:
        put.wait()


def finish_call(*parts):
    hbm = pl.BlockSpec(memory_space=pl.ANY)
    return pl.pallas_call(
        finish,
        out_shape=(
            jax.ShapeDtypeStruct((384, 2048), BF16),
            jax.ShapeDtypeStruct((128, 1024), F32),
            jax.ShapeDtypeStruct((128, 1024), F32),
            jax.ShapeDtypeStruct((16, 128, 128), F32),
            jax.ShapeDtypeStruct((16, 128), F32),
            jax.ShapeDtypeStruct((8, 128), F32),
            jax.ShapeDtypeStruct((8, 128), F32),
        ),
        in_specs=[hbm] * 6,
        out_specs=(hbm,) * 7,
        scratch_shapes=[
            pltpu.VMEM((384, 2048), BF16),
            pltpu.VMEM((2, 128, 1024), BF16),
            pltpu.VMEM((2, 128, 1024), F32),
            pltpu.VMEM((16, 128, 128), BF16),
            pltpu.VMEM((16, 128, 128), F32),
            pltpu.VMEM((16, 128), F32),
            pltpu.VMEM((8, 128), F32),
            pltpu.VMEM((8, 128), F32),
            pltpu.SemaphoreType.DMA((10,)),
            pltpu.SemaphoreType.DMA((10,)),
        ],
        name="finish",
    )(*parts)


def shards(tokens, value_act, gate_act, cotangent, value_weight, gate_weight,
           norm_gain, norm_bias, mix_weight, mix_bias):
    parts = fused_call(
        tokens[0], value_act[0], gate_act[0], cotangent[0], value_weight, gate_weight,
        mix_weight, norm_gain[None], norm_bias[None], mix_bias)
    tgrad, vout, gout, mout, bout, nout, hout = finish_call(*parts)
    return tgrad[None], vout, gout, mout, bout, nout.reshape(1024), hout.reshape(1024)


def solution(mesh):
    rows = P("dp", "sp", None)
    placed = (rows, rows, rows, rows, P("dp", None), P("dp", None), P(), P(), P(), P())
    return jax.shard_map(
        shards, mesh=mesh, in_specs=placed,
        out_specs=(rows, P("dp", None), P("dp", None), P(), P(), P(), P()), check_vma=False)
```

time: 604 us -> 75.5 us (0.12)
  waiting for transfers between devices: 426 us -> 0 us
  blocking collectives: 80.6 us -> 0 us
  Pallas kernels: 0 us -> 74.7 us
  local copies, waits for them, and re-layouts: 36.4 us -> 0 us
  matrix products: 25.3 us -> 0 us
  other arithmetic: 19.3 us -> 0 us
  between operations: 14 us -> 0.64 us
    psum x2 -> x0, waiting for transfers between devices: 326 us -> none  [the longest x1 261 us: shards(): totals = lax.psum((stats[0], stats[1], stats[2], stats[3]), ('sp', 'dp'))]
    reduce_scatter x1 -> x0, waiting for transfers between devices: 101 us -> none  [shards(): lax.psum_scatter(lax.dot_general(inputs, both_grads, (((0,), (0,)), ((),...]
    psum x1 -> x0, blocking collectives: 80.6 us -> none  [shards(): totals = lax.psum((stats[0], stats[1], stats[2], stats[3]), ('sp', 'dp'))]
    pallas_call x0 -> x2, Pallas kernels: none -> 74.7 us  [the longest x1 71.7 us: fused_call(): pl.pallas_call(fused, out_shape=(jax.ShapeDtypeStruct((384, 2048), BF16),...]
    dot_general x5 -> x0, matrix products: 25.3 us -> none  [the longest x1 9.36 us: shards(): lax.dot_general(inputs, both_grads, (((0,), (0,)), ((), ())), preferred_e...]
    unnamed x40 -> x0, local copies, waits for them, and re-layouts: 14.9 us -> none
    mul x5 -> x0, local copies, waits for them, and re-layouts: 14.4 us -> none  [the longest x2 7.21 us: mixer_backward(): gate_gelu = jax.nn.gelu(gate_float, approximate=False)]
    reduce_sum x3 -> x0, other arithmetic: 10.4 us -> none  [the longest x1 5.61 us: mixer_backward(): bias_grad = jnp.sum(grad_split, axis=(0, 3)).T]
  transfers between devices with their start and end apart: 4 -> 0, of which waited for: 3 -> 0; matrix products, arithmetic and copies ran while one was open for 3% -> 0% of each run, Pallas kernels for 0% -> 0%
where the time goes in v2:
time: 75.5 us; the launch traced here: 75.3 us
  Pallas kernels  74.7 us (99%)
    pallas_call x1, Pallas kernels, fused_call(): pl.pallas_call(fused, out_shape=(jax.ShapeDtypeStruct((384, 2048), BF16),...  71.7 us
    pallas_call x1, Pallas kernels, finish_call(): pl.pallas_call(finish, out_shape=(jax.ShapeDtypeStruct((384, 2048), BF16)...  3 us

profile of v2, /device:TPU:1, one launch (start us, length us, event | category | flops | bytes accessed | tf_op | source)
XLA Modules:
  0.0 75.3 jit_solution(16171962147261238726)
XLA Ops:
  0.6 71.7 %fused.1 = (bf16[384,2048]{1,0:T(8,128)(2,1)}, bf16[2,128,1024]{2,1,0:T(8,128)(2,1)}, bf16[16,128,128]{2,1,0:T(8,128)(2,1)}, f32[16,128]{1,0:T(8,128)}, f32[8,128]{1,0:T(8,128)}, /*index=5*/f32[8,128]{1,0:T(8,128)}) custom-call(bf16[384,2048]{1,0:T(8,128)(2,1)} %bitcast.9, bf16[384,1024]{1,0:T(8,128)(2,1)} %bitcast.10, bf16[384,1024]{1,0:T(8,128)(2,1)} %bitcast.11, ...), custom_call_target="tpu_custom_call" | custom-call | tf_op jit(solution)/shard_map/fused/pallas_call | solution.py:733
  72.3 3.0 %finish.1 = (bf16[384,2048]{1,0:T(8,128)(2,1)}, f32[128,1024]{1,0:T(8,128)}, f32[128,1024]{1,0:T(8,128)}, f32[16,128,128]{2,1,0:T(8,128)}, f32[16,128]{1,0:T(8,1...) custom-call(bf16[384,2048]{1,0:T(8,128)(2,1)} %get-tuple-element.20.tgrad, bf16[2,128,1024]{2,1,0:T(8,128)(2,1)} %get-tuple-element.21.wsum, ...), custom_call_target="tpu_custom_call" | custom-call | tf_op jit(solution)/shard_map/finish/pallas_call | solution.py:784

commit v3 on v2

--- a/solution.py
+++ b/solution.py
@@ -50,7 +50,6 @@
 
 
 def fused(tokens, va_h, ga_h, cot_h, vw, gw, mixw_h, gain_h, bias_h, mixb_h,
-          tgrad_h, wout_h, mixo_h, bout_h, nout_h, hout_h,
           tgrad, wout, mixo, bout, nout, hout, gain, bias, mixb,
           va, ga, cot, mixw, tokl, mcat, mtrn, normed, slope, spread, low, cv, gnorm, inv, gsum, bfull, acc_g, acc_b,
           grads, wgrad, stats,
@@ -58,7 +57,7 @@
           sfar, sup, sdn, fup, fdn, own1, agg, rlay, rprev, rnext, s1f, s1b, r2, own2, s2b, r3, fin, allf,
           mrecv, mq, mqb, mr1, mq1, mq1b, mr2, my, maz, max_, macc, mpart, mrp,
           stc, stx, sty, stz, stg, st0, st1,
-          loc, outs, tok_s, tok_r, grd_s, grd_r, ring_s, ring_r, help_s, help_r, pair_s, pair_r, one_s, one_r, two_s, two_r,
+          loc, tok_s, tok_r, grd_s, grd_r, ring_s, ring_r, help_s, help_r, pair_s, pair_r, one_s, one_r, two_s, two_r,
           thr_s, thr_r, fou_s, fou_r, mix_s, mix_r, sts_s, sts_r):
     sp = lax.axis_index("sp")
     dp = lax.axis_index("dp")
@@ -112,7 +111,7 @@
     local.append(pltpu.make_async_copy(gain_h, gain, loc.at[14]))
     local.append(pltpu.make_async_copy(bias_h, bias, loc.at[15]))
     local.append(pltpu.make_async_copy(mixb_h, mixb, loc.at[16]))
-    for n in (0, 1, 2, 14, 15, 16, 13, 5, 6, 7, 8, 9, 10, 11, 12, 3, 4):
+    for n in (13, 16, 0, 1, 2, 14, 15, 5, 6, 7, 8, 9, 10, 11, 12, 3, 4):
         local[n].start()
 
     axes = ("x", "y")
@@ -209,6 +208,35 @@
     gsum[...] = jnp.zeros_like(gsum)
     acc_g[...] = jnp.zeros_like(acc_g)
     acc_b[...] = jnp.zeros_like(acc_b)
+    mark("m_prep")
+    local[13].wait()
+    def prep(p, _):
+        for h in range(2):
+            m = jnp.where(keep, mixw[2 * p + h].astype(F32), 0.0)
+            mcat[p, :, h * 128:(h + 1) * 128] = m.astype(BF16)
+            mtrn[p, :, h * 128:(h + 1) * 128] = m.T.astype(BF16)
+        return 0
+
+    lax.fori_loop(0, 8, prep, 0)
+    group = lax.broadcasted_iota(jnp.int32, (16, 1024), 0)
+    chan = lax.broadcasted_iota(jnp.int32, (16, 1024), 1) // 64
+    pick = jnp.where(group == chan, 1.0, 0.0).astype(BF16)
+    local[16].wait()
+    parts = split3(mixb[...])
+    bfull[...] = dot(parts[0], pick, TN) + dot(parts[1], pick, TN) + dot(parts[2], pick, TN)
+
+    mark("barrierwait")
+    pl.semaphore_wait(barrier, 23)
+    for part in (1, 0):
+        for v in range(2):
+            for direction in range(2):
+                hop(direction, v, 1, part).start()
+    for k in range(8):
+        lanes = pl.ds(pl.multiple_of((2 * k + pc) * 128, 128), 128)
+        copy(tokens.at[:, lanes], tokr.at[k], tok_s.at[0], tok_r.at[0], at(nc=pc)).start()
+    for v in range(2):
+        copy(shard[v], wbuf.at[z, v, c], pair_s.at[v], pair_r.at[v], at(nc=pc)).start()
+
     mark("m_value")
     local[0].wait()
     local[1].wait()
@@ -225,18 +253,6 @@
         return 0
 
     lax.fori_loop(0, 24, first, 0)
-
-    mark("barrierwait")
-    pl.semaphore_wait(barrier, 23)
-    for part in (1, 0):
-        for v in range(2):
-            for direction in range(2):
-                hop(direction, v, 1, part).start()
-    for k in range(8):
-        lanes = pl.ds(pl.multiple_of((2 * k + pc) * 128, 128), 128)
-        copy(tokens.at[:, lanes], tokr.at[k], tok_s.at[0], tok_r.at[0], at(nc=pc)).start()
-    for v in range(2):
-        copy(shard[v], wbuf.at[z, v, c], pair_s.at[v], pair_r.at[v], at(nc=pc)).start()
 
     mark("m_gate")
     local[2].wait()
@@ -259,23 +275,6 @@
 
     lax.fori_loop(0, 24 // GATE_UNROLL, second, 0)
 
-    mark("m_prep")
-    local[13].wait()
-    def prep(p, _):
-        for h in range(2):
-            m = jnp.where(keep, mixw[2 * p + h].astype(F32), 0.0)
-            mcat[p, :, h * 128:(h + 1) * 128] = m.astype(BF16)
-            mtrn[p, :, h * 128:(h + 1) * 128] = m.T.astype(BF16)
-        return 0
-
-    lax.fori_loop(0, 8, prep, 0)
-    group = lax.broadcasted_iota(jnp.int32, (16, 1024), 0)
-    chan = lax.broadcasted_iota(jnp.int32, (16, 1024), 1) // 64
-    pick = jnp.where(group == chan, 1.0, 0.0).astype(BF16)
-    local[16].wait()
-    parts = split3(mixb[...])
-    bfull[...] = dot(parts[0], pick, TN) + dot(parts[1], pick, TN) + dot(parts[2], pick, TN)
-
     mark("transpose")
     for k in range(8):
         local[5 + k].wait()
@@ -292,7 +291,7 @@
     m0 = jnp.where(lane < 64, 1.0, 0.0).astype(BF16)
     m1 = jnp.where(lane < 64, 0.0, 1.0).astype(BF16)
 
-    def mix(p, _):
+    def mix_pair(p):
         cols = pl.ds(pl.multiple_of(p * 128, 128), 128)
         wg = None
         for b in range(3):
@@ -308,15 +307,26 @@
             wg = term if wg is None else wg + term
         wgrad[2 * p] = jnp.where(keep, wg[:128], 0.0)
         wgrad[2 * p + 1] = jnp.where(keep, wg[128:], 0.0)
+
+    reach = (2, 1, 3, 0)
+
+    def swap(h, j):
+        dest = lax.rem(place[h] + reach[j], 4)
+        lanes = pl.ds(pl.multiple_of(h * 1024 + dest * 256, 256), 256)
+        return copy(grads.at[pl.ds(0, 384), lanes], grads.at[pl.ds(384, 384), lanes],
+                    grd_s.at[h * 4 + j], grd_r.at[h * 4 + j], at(nc=pc))
+
+    def mix(j, _):
+        dest = lax.rem(x + 2 + j, 4)
+        mix_pair(2 * dest)
+        mix_pair(2 * dest + 1)
         return 0
 
-    lax.fori_loop(0, 8, mix, 0)
-
-    def swap(h):
-        lanes = pl.ds(h * 1024, 1024)
-        return copy(grads.at[pl.ds(0, 384), lanes], grads.at[pl.ds(384, 384), lanes], grd_s.at[h], grd_r.at[h], at(nc=pc))
-
-    swap(0).start()
+    mix(0, 0)
+    swap(0, 0).start()
+    lax.fori_loop(1, 4, mix, 0)
+    for j in (1, 2, 3):
+        swap(0, j).start()
     for k in range(8):
         copy(wgrad.at[2 * k + pc], mrecv.at[k], mix_s.at[0], mix_r.at[0], at(nc=pc)).start()
 
@@ -338,54 +348,73 @@
         return 0
 
     lax.fori_loop(0, 24 // LAST_UNROLL, last, 0)
-    swap(1).start()
-    mark("m_stats")
-    parts = split3(gsum[...])
-    stats[0:16, :] = dot(pick, parts[0], NT) + dot(pick, parts[1], NT) + dot(pick, parts[2], NT)
-    tot_g = jnp.sum(acc_g[...], axis=0, keepdims=True)
-    tot_b = jnp.sum(acc_b[...], axis=0, keepdims=True)
-    for k in range(8):
-        stats[16 + k:17 + k, :] = tot_g[:, k * 128:(k + 1) * 128]
-        stats[24 + k:25 + k, :] = tot_b[:, k * 128:(k + 1) * 128]
-    copy(stats, stc, sts_s.at[0], sts_r.at[0], at(nc=pc)).start()
-    def product(h, dest, half):
+    for j in range(4):
+        swap(1, j).start()
+    def stats_pair():
+        mark("m_stats")
+        parts = split3(gsum[...])
+        stats[0:16, :] = dot(pick, parts[0], NT) + dot(pick, parts[1], NT) + dot(pick, parts[2], NT)
+        tot_g = jnp.sum(acc_g[...], axis=0, keepdims=True)
+        tot_b = jnp.sum(acc_b[...], axis=0, keepdims=True)
+        for k in range(8):
+            stats[16 + k:17 + k, :] = tot_g[:, k * 128:(k + 1) * 128]
+            stats[24 + k:25 + k, :] = tot_b[:, k * 128:(k + 1) * 128]
+        copy(stats, stc, sts_s.at[0], sts_r.at[0], at(nc=pc)).start()
+
+    def product(h, j, half):
+        swap_in(h, j)
+        dest = lax.rem(place[h] + reach[j], 4)
         wide = pl.ds(pl.multiple_of(h * 1024 + dest * 256, 256), 256)
-        return dot(tt[half * 512:(half + 1) * 512, :], grads[:, wide]).reshape(2, 256, 256)
-
-    def one(i, h, src, dst, k):
-        return copy(src, dst, one_s.at[h * 6 + i], one_r.at[h * 6 + i], along(axes[h], k))
+        v = dot(tt[half * 512:(half + 1) * 512, :], grads[:, wide])
+        return v[:, :128], v[:, 128:]
+
+    arrived = set()
+
+    def swap_in(h, j):
+        if (h, j) not in arrived:
+            arrived.add((h, j))
+            swap(h, j).wait_recv()
+
+    def one(i, g, src, dst, k):
+        return copy(src, dst, one_s.at[g * 6 + i], one_r.at[g * 6 + i], along(axes[g // 2], k))
 
     def far_tiles(h):
         mark(f"far{h}")
-        dest = lax.rem(place[h] + 2, 4)
-        sfar[h, 0:2] = product(h, dest, 0).astype(BF16)
-        one(0, h, sfar.at[h, 0:2], rlay.at[h, 0], 1).start()
-        sfar[h, 2:4] = product(h, dest, 1).astype(BF16)
-        one(1, h, sfar.at[h, 2:4], rlay.at[h, 1], 3).start()
+        for half, k in ((0, 1), (1, 3)):
+            v = product(h, 0, half)
+            for n in range(2):
+                g = 2 * h + n
+                sfar[g, half] = v[n].astype(BF16)
+                one(half, g, sfar.at[g, half], rlay.at[g, half], k).start()
 
     def near_tiles(h):
         mark(f"near{h}")
-        up, dn = lax.rem(place[h] + 1, 4), lax.rem(place[h] + 3, 4)
-        sup[h, 2:4] = product(h, up, 1).astype(BF16)
-        one(2, h, sup.at[h, 2:4], rprev.at[h, 1], 1).start()
-        sdn[h, 0:2] = product(h, dn, 0).astype(BF16)
-        one(3, h, sdn.at[h, 0:2], rnext.at[h, 0], 3).start()
-        fup[h, 0:2] = product(h, up, 0)
-        fdn[h, 2:4] = product(h, dn, 1)
+        v = product(h, 1, 1)
+        for n in range(2):
+            g = 2 * h + n
+            sup[g] = v[n].astype(BF16)
+            one(2, g, sup.at[g], rprev.at[g, 1], 1).start()
+        v = product(h, 2, 0)
+        for n in range(2):
+            g = 2 * h + n
+            sdn[g] = v[n].astype(BF16)
+            one(3, g, sdn.at[g], rnext.at[g, 0], 3).start()
+        fup[2 * h], fup[2 * h + 1] = product(h, 1, 0)
+        fdn[2 * h], fdn[2 * h + 1] = product(h, 2, 1)
 
     def own_tiles(h):
         mark(f"own{h}")
-        own1[h, 0:2] = product(h, place[h], 0)
-        own1[h, 2:4] = product(h, place[h], 1)
-
-    def relay(h):
-        mark(f"relay{h}")
-        one(0, h, rlay.at[h, 0], rlay.at[h, 0], 1).wait_recv()
-        agg[h, 0] = (fup[h, 0:2] + rlay[h, 0].astype(F32)).astype(BF16)
-        one(4, h, agg.at[h, 0], rprev.at[h, 0], 1).start()
-        one(1, h, rlay.at[h, 1], rlay.at[h, 1], 3).wait_recv()
-        agg[h, 1] = (fdn[h, 2:4] + rlay[h, 1].astype(F32)).astype(BF16)
-        one(5, h, agg.at[h, 1], rnext.at[h, 1], 3).start()
+        for half in range(2):
+            own1[2 * h, half], own1[2 * h + 1, half] = product(h, 3, half)
+
+    def relay(g):
+        mark(f"relay{g}")
+        one(0, g, rlay.at[g, 0], rlay.at[g, 0], 1).wait_recv()
+        agg[g, 0] = (fup[g] + rlay[g, 0].astype(F32)).astype(BF16)
+        one(4, g, agg.at[g, 0], rprev.at[g, 0], 1).start()
+        one(1, g, rlay.at[g, 1], rlay.at[g, 1], 3).wait_recv()
+        agg[g, 1] = (fdn[g] + rlay[g, 1].astype(F32)).astype(BF16)
+        one(5, g, agg.at[g, 1], rnext.at[g, 1], 3).start()
 
     def stats_x():
         mark("stats_x")
@@ -428,35 +457,32 @@
         bout[8:16] = stg[1]
         nout[...] = stg[2]
         hout[...] = stg[3]
-        for n in (3, 4, 5):
-            put[n].start()
+
+    def mix_x():
+        mark("mix_x")
+        await_recv(mrecv, mix_s.at[0], mix_r.at[0])
+        for k in range(8):
+            v = (wgrad[2 * k + c] + mrecv[k]).reshape(4, 32, 128)
+            mq[k] = v
+            mqb[k] = v.astype(BF16)
+        for k in range(1, 4):
+            copy(mqb.at[:, lax.rem(x + k, 4)], mr1.at[k - 1], mix_s.at[1], mix_r.at[1], along("x", k)).start()
 
     def mix_z():
         mark("mix_z")
-        await_recv(mrecv, mix_s.at[0], mix_r.at[0])
-        for k in range(8):
-            v = wgrad[2 * k + c] + mrecv[k]
-            mq[k] = v
-            mqb[k] = v.astype(BF16)
+        await_recv(mr1, mix_s.at[1], mix_r.at[1])
+        v = mq[:, x] + (mr1[0].astype(F32) + mr1[1].astype(F32)) + mr1[2].astype(F32)
+        mq1[...] = v
+        mq1b[...] = v.astype(BF16)
         for k in range(1, 8):
-            copy(mqb.at[lax.rem(z + k, 8)], mr2.at[k - 1], mix_s.at[1], mix_r.at[1], along("z", k)).start()
-
-    def mix_x():
-        mark("mix_x")
-        await_recv(mr2, mix_s.at[1], mix_r.at[1])
-        v = mq[z]
+            copy(mq1b.at[lax.rem(z + k, 8)], mr2.at[k - 1], mix_s.at[2], mix_r.at[2], along("z", k)).start()
+
+    def mix_y():
+        mark("mix_y")
+        await_recv(mr2, mix_s.at[2], mix_r.at[2])
+        v = mq1[z]
         for k in range(7):
             v = v + mr2[k].astype(F32)
-        v = v.reshape(4, 32, 128)
-        mq1[...] = v
-        mq1b[...] = v.astype(BF16)
-        for k in range(1, 4):
-            copy(mq1b.at[lax.rem(x + k, 4)], mr1.at[k - 1], mix_s.at[2], mix_r.at[2], along("x", k)).start()
-
-    def mix_y():
-        mark("mix_y")
-        await_recv(mr1, mix_s.at[2], mix_r.at[2])
-        v = mq1[x] + (mr1[0].astype(F32) + mr1[1].astype(F32)) + mr1[2].astype(F32)
         mpart[...] = v
         my[y] = v
         for k in range(1, 4):
@@ -489,7 +515,6 @@
         for k in range(8):
             mixo[2 * k + c] = max_[:, k].reshape(128, 128)
             mixo[2 * k + pc] = mrp[:, k].reshape(128, 128)
-        put[2].start()
 
     def ring(h, v):
         mark(f"ring{h}{v}")
@@ -507,123 +532,121 @@
         if h < 4:
             into_tokens(lax.rem(z + 8 - h, 8))
 
-    put = [pltpu.make_async_copy(tgrad, tgrad_h, outs.at[0]), pltpu.make_async_copy(wout.at[0], wout_h.at[0], outs.at[1]),
-           pltpu.make_async_copy(mixo, mixo_h, outs.at[2]), pltpu.make_async_copy(bout, bout_h, outs.at[3]),
-           pltpu.make_async_copy(nout, nout_h, outs.at[4]), pltpu.make_async_copy(hout, hout_h, outs.at[5]),
-           pltpu.make_async_copy(wout.at[1], wout_h.at[1], outs.at[6])]
-
-    def stage_two(h):
-        mark(f"two{h}")
-        for i, buf in ((2, rprev.at[h, 1]), (4, rprev.at[h, 0]), (3, rnext.at[h, 0]), (5, rnext.at[h, 1])):
-            one(i, h, buf, buf, 1).wait_recv()
-        for q in range(4):
-            v = own1[h, q] + (rprev[h, q // 2, q % 2].astype(F32) + rnext[h, q // 2, q % 2].astype(F32))
-            v = v.reshape(2, 4, 32, 256)
-            s1f[h, 2 * q:2 * q + 2] = v
-            s1b[h, 2 * q:2 * q + 2] = v.astype(BF16)
+    def stage_two(g):
+        mark(f"two{g}")
+        for i, buf in ((2, rprev.at[g, 1]), (3, rnext.at[g, 0]), (4, rprev.at[g, 0]), (5, rnext.at[g, 1])):
+            one(i, g, buf, buf, 1).wait_recv()
+        for q in range(2):
+            v = own1[g, q] + (rprev[g, q].astype(F32) + rnext[g, q].astype(F32))
+            v = v.reshape(4, 4, 32, 128)
+            s1f[g, 4 * q:4 * q + 4] = v
+            s1b[g, 4 * q:4 * q + 4] = v.astype(BF16)
+        h = g // 2
         other = place[1 - h]
-        for k in range(1, 4):
-            copy(s1b.at[h, :, lax.rem(other + k, 4)], r2.at[h, k - 1], two_s.at[h], two_r.at[h],
+        for k in (2, 1, 3):
+            copy(s1b.at[g, :, lax.rem(other + k, 4)], r2.at[g, k - 1], two_s.at[g], two_r.at[g],
                  along(axes[1 - h], k)).start()
 
-    def stage_three(h):
-        mark(f"three{h}")
-        await_recv(r2.at[h], two_s.at[h], two_r.at[h])
-        v = s1f[h, :, place[1 - h]] + (r2[h, 0].astype(F32) + r2[h, 1].astype(F32)) + r2[h, 2].astype(F32)
-        own2[h] = v
-        s2b[h] = v.astype(BF16)
-        for k in range(1, 8):
-            copy(s2b.at[h, lax.rem(z + k, 8)], r3.at[h, k - 1], thr_s.at[h], thr_r.at[h], along("z", k)).start()
-
-    def stage_four(h):
-        mark(f"four{h}")
-        await_recv(r3.at[h], thr_s.at[h], thr_r.at[h])
-        v = own2[h, z]
+    def stage_three(g):
+        mark(f"three{g}")
+        await_recv(r2.at[g], two_s.at[g], two_r.at[g])
+        v = s1f[g, :, place[1 - g // 2]] + (r2[g, 0].astype(F32) + r2[g, 1].astype(F32)) + r2[g, 2].astype(F32)
+        own2[g] = v
+        s2b[g] = v.astype(BF16)
+        for k in (4, 3, 5, 2, 6, 1, 7):
+            copy(s2b.at[g, lax.rem(z + k, 8)], r3.at[g, k - 1], thr_s.at[g], thr_r.at[g], along("z", k)).start()
+
+    def stage_four(g):
+        mark(f"four{g}")
+        await_recv(r3.at[g], thr_s.at[g], thr_r.at[g])
+        v = own2[g, z]
         for k in range(7):
-            v = v + r3[h, k].astype(F32)
-        fin[h] = v.astype(BF16)
-        allf[h, sp] = v.astype(BF16)
+            v = v + r3[g, k].astype(F32)
+        fin[g] = v.astype(BF16)
+        allf[g, sp] = v.astype(BF16)
         for k in range(1, 16):
-            copy(fin.at[h], allf.at[h, sp], fou_s.at[h], fou_r.at[h], {"sp": lax.rem(sp + k, 16), "dp": dp}).start()
-
-    def stage_end(h):
-        mark(f"end{h}")
-        await_recv(allf.at[h, pl.ds(0, 15)], fou_s.at[h], fou_r.at[h])
+            copy(fin.at[g], allf.at[g, sp], fou_s.at[g], fou_r.at[g], {"sp": lax.rem(sp + k, 16), "dp": dp}).start()
+
+    def stage_end(g):
+        mark(f"end{g}")
+        await_recv(allf.at[g, pl.ds(0, 15)], fou_s.at[g], fou_r.at[g])
+        h, n = g // 2, g % 2
         for s in range(16):
             a, b = (s // 4, s % 4) if h == 0 else (s % 4, s // 4)
-            wout[h, a * 32:(a + 1) * 32, b * 256:(b + 1) * 256] = allf[h, s]
-        put[(1, 6)[h]].start()
-
-    swap(0).wait_recv()
+            wout[h, a * 32:(a + 1) * 32, b * 256 + n * 128:b * 256 + (n + 1) * 128] = allf[g, s]
+
     far_tiles(0)
     ring(1, 0)
-    swap(1).wait_recv()
+    mix_x()
+    stats_pair()
     far_tiles(1)
-    mix_z()
+    near_tiles(0)
     ring(1, 1)
-    near_tiles(0)
     near_tiles(1)
-    stats_x()
+    help_pair(1)
     own_tiles(0)
     own_tiles(1)
-    relay(0)
-    relay(1)
+    stats_x()
+    for g in range(4):
+        relay((0, 2, 1, 3)[g])
     ring(2, 0)
     into(0)
+    mix_z()
+    into(1)
+    stats_y()
     ring(2, 1)
-    help_pair(1)
-    into(1)
+    stage_two(0)
     ring(3, 0)
-    stage_two(0)
+    stage_two(2)
+    mix_y()
     stage_two(1)
-    stats_y()
-    mix_x()
+    stage_two(3)
+    ring(3, 1)
+    stats_z()
     for v in range(2):
         help_out(2, v)
-    ring(3, 1)
+    mix_back_z()
     stage_three(0)
+    stage_three(2)
     stage_three(1)
-    mix_y()
-    stats_z()
-    for v in range(2):
-        help_out(3, v)
-    mark("help_pair2")
-    help_pair(2)
-    into(2)
+    stage_three(3)
     ring(4, 0)
     ring(4, 1)
     for v in range(2):
+        help_out(3, v)
         help_out(4, v)
-    mix_back_z()
+    mark("help_pair2")
+    help_pair(2)
+    mix_back_x()
     stage_four(0)
+    stage_four(2)
     stage_four(1)
+    stage_four(3)
+    stats_back()
+    into(2)
     mark("help_pair3")
     help_pair(3)
+    help_pair(4)
     into(3)
-    mix_back_x()
-    stats_back()
-    mark("help_pair4")
-    help_pair(4)
+    mix_back_c()
     into(4)
-    put[0].start()
-    mix_back_c()
+    mix_end()
     stats_end()
-    mix_end()
-    stage_end(0)
-    stage_end(1)
+    for g in (0, 2, 1, 3):
+        stage_end(g)
 
     mark("sends")
-    for one_out in put:
-        one_out.wait()
     await_send(tokr, tok_s.at[0], tok_r.at[0])
     for h in range(2):
-        swap(h).wait_send()
+        for j in range(4):
+            swap(h, j).wait_send()
+    for g in range(4):
         for i in range(6):
-            await_send(agg.at[h, 0], one_s.at[h * 6 + i], one_r.at[h * 6 + i])
-        await_send(r2.at[h], two_s.at[h], two_r.at[h])
-        await_send(r3.at[h], thr_s.at[h], thr_r.at[h])
-        await_send(allf.at[h, pl.ds(0, 15)], fou_s.at[h], fou_r.at[h])
-    for i, buf in enumerate((mrecv, mr2, mr1, my.at[pl.ds(0, 3)], maz.at[pl.ds(0, 7)],
+            await_send(sup.at[g], one_s.at[g * 6 + i], one_r.at[g * 6 + i])
+        await_send(r2.at[g], two_s.at[g], two_r.at[g])
+        await_send(r3.at[g], thr_s.at[g], thr_r.at[g])
+        await_send(allf.at[g, pl.ds(0, 15)], fou_s.at[g], fou_r.at[g])
+    for i, buf in enumerate((mrecv, mr1, mr2, my.at[pl.ds(0, 3)], maz.at[pl.ds(0, 7)],
                              max_.at[pl.ds(0, 3)], mrp)):
         await_send(buf, mix_s.at[i], mix_r.at[i])
     for i, buf in enumerate((stc, stx, sty.at[pl.ds(0, 3)], stz.at[pl.ds(0, 7)], stg.at[pl.ds(0, 3)])):
@@ -642,12 +665,6 @@
 
 
 SCRATCH = (
-    pltpu.VMEM((384, 2048), BF16),
-    pltpu.VMEM((2, 128, 1024), BF16),
-    pltpu.VMEM((16, 128, 128), BF16),
-    pltpu.VMEM((16, 128), F32),
-    pltpu.VMEM((8, 128), F32),
-    pltpu.VMEM((8, 128), F32),
     pltpu.VMEM((1, 1024), F32),
     pltpu.VMEM((1, 1024), F32),
     pltpu.VMEM((16, 128), F32),
@@ -675,31 +692,31 @@
     pltpu.VMEM((8, 384, 128), BF16),
     pltpu.VMEM((1024, 768), BF16),
     pltpu.VMEM((8, 2, 2, 128, 1024), BF16),
-    pltpu.VMEM((2, 4, 256, 256), BF16),
-    pltpu.VMEM((2, 4, 256, 256), BF16),
-    pltpu.VMEM((2, 4, 256, 256), BF16),
-    pltpu.VMEM((2, 4, 256, 256), F32),
-    pltpu.VMEM((2, 4, 256, 256), F32),
-    pltpu.VMEM((2, 4, 256, 256), F32),
-    pltpu.VMEM((2, 2, 2, 256, 256), BF16),
-    pltpu.VMEM((2, 2, 2, 256, 256), BF16),
-    pltpu.VMEM((2, 2, 2, 256, 256), BF16),
-    pltpu.VMEM((2, 2, 2, 256, 256), BF16),
-    pltpu.VMEM((2, 8, 4, 32, 256), F32),
-    pltpu.VMEM((2, 8, 4, 32, 256), BF16),
-    pltpu.VMEM((2, 3, 8, 32, 256), BF16),
-    pltpu.VMEM((2, 8, 32, 256), F32),
-    pltpu.VMEM((2, 8, 32, 256), BF16),
-    pltpu.VMEM((2, 7, 32, 256), BF16),
-    pltpu.VMEM((2, 32, 256), BF16),
-    pltpu.VMEM((2, 16, 32, 256), BF16),
+    pltpu.VMEM((4, 2, 512, 128), BF16),
+    pltpu.VMEM((4, 512, 128), BF16),
+    pltpu.VMEM((4, 512, 128), BF16),
+    pltpu.VMEM((4, 512, 128), F32),
+    pltpu.VMEM((4, 512, 128), F32),
+    pltpu.VMEM((4, 2, 512, 128), F32),
+    pltpu.VMEM((4, 2, 512, 128), BF16),
+    pltpu.VMEM((4, 2, 512, 128), BF16),
+    pltpu.VMEM((4, 2, 512, 128), BF16),
+    pltpu.VMEM((4, 2, 512, 128), BF16),
+    pltpu.VMEM((4, 8, 4, 32, 128), F32),
+    pltpu.VMEM((4, 8, 4, 32, 128), BF16),
+    pltpu.VMEM((4, 3, 8, 32, 128), BF16),
+    pltpu.VMEM((4, 8, 32, 128), F32),
+    pltpu.VMEM((4, 8, 32, 128), BF16),
+    pltpu.VMEM((4, 7, 32, 128), BF16),
+    pltpu.VMEM((4, 32, 128), BF16),
+    pltpu.VMEM((4, 16, 32, 128), BF16),
     pltpu.VMEM((8, 128, 128), F32),
-    pltpu.VMEM((8, 128, 128), F32),
-    pltpu.VMEM((8, 128, 128), BF16),
-    pltpu.VMEM((3, 32, 128), BF16),
-    pltpu.VMEM((4, 32, 128), F32),
-    pltpu.VMEM((4, 32, 128), BF16),
-    pltpu.VMEM((7, 128, 128), BF16),
+    pltpu.VMEM((8, 4, 32, 128), F32),
+    pltpu.VMEM((8, 4, 32, 128), BF16),
+    pltpu.VMEM((3, 8, 32, 128), BF16),
+    pltpu.VMEM((8, 32, 128), F32),
+    pltpu.VMEM((8, 32, 128), BF16),
+    pltpu.VMEM((7, 32, 128), BF16),
     pltpu.VMEM((4, 32, 128), F32),
     pltpu.VMEM((8, 32, 128), BF16),
     pltpu.VMEM((4, 8, 32, 128), BF16),
@@ -713,74 +730,60 @@
     pltpu.VMEM((4, 8, 128), F32),
     pltpu.VMEM((4, 8, 128), F32),
     pltpu.VMEM((3, 8, 128), F32),
-    pltpu.SemaphoreType.DMA((17,)), pltpu.SemaphoreType.DMA((7,)),
+    pltpu.SemaphoreType.DMA((17,)),
     pltpu.SemaphoreType.DMA((1,)), pltpu.SemaphoreType.DMA((1,)),
-    pltpu.SemaphoreType.DMA((2,)), pltpu.SemaphoreType.DMA((2,)),
+    pltpu.SemaphoreType.DMA((8,)), pltpu.SemaphoreType.DMA((8,)),
     pltpu.SemaphoreType.DMA((32,)), pltpu.SemaphoreType.DMA((32,)),
     pltpu.SemaphoreType.DMA((16,)), pltpu.SemaphoreType.DMA((16,)),
     pltpu.SemaphoreType.DMA((34,)), pltpu.SemaphoreType.DMA((34,)),
-    pltpu.SemaphoreType.DMA((12,)), pltpu.SemaphoreType.DMA((12,)),
-    pltpu.SemaphoreType.DMA((2,)), pltpu.SemaphoreType.DMA((2,)),
-    pltpu.SemaphoreType.DMA((2,)), pltpu.SemaphoreType.DMA((2,)),
-    pltpu.SemaphoreType.DMA((2,)), pltpu.SemaphoreType.DMA((2,)),
+    pltpu.SemaphoreType.DMA((24,)), pltpu.SemaphoreType.DMA((24,)),
+    pltpu.SemaphoreType.DMA((4,)), pltpu.SemaphoreType.DMA((4,)),
+    pltpu.SemaphoreType.DMA((4,)), pltpu.SemaphoreType.DMA((4,)),
+    pltpu.SemaphoreType.DMA((4,)), pltpu.SemaphoreType.DMA((4,)),
     pltpu.SemaphoreType.DMA((7,)), pltpu.SemaphoreType.DMA((7,)),
     pltpu.SemaphoreType.DMA((5,)), pltpu.SemaphoreType.DMA((5,)),
 )
 
 
 def fused_call(tokens, va, ga, cot, vw, gw, mixw, gain, bias, mixb):
-    hbm = pl.BlockSpec(memory_space=pl.ANY)
+    hbm = pl.BlockSpec(memory_space=pltpu.HBM)
+    vm = pl.BlockSpec(memory_space=pltpu.VMEM)
     return pl.pallas_call(
         fused,
         out_shape=(
-            jax.ShapeDtypeStruct((384, 2048), BF16),
-            jax.ShapeDtypeStruct((2, 128, 1024), BF16),
-            jax.ShapeDtypeStruct((16, 128, 128), BF16),
-            jax.ShapeDtypeStruct((16, 128), F32),
-            jax.ShapeDtypeStruct((8, 128), F32),
-            jax.ShapeDtypeStruct((8, 128), F32),
+            pltpu.VMEM((384, 2048), BF16),
+            pltpu.VMEM((2, 128, 1024), BF16),
+            pltpu.VMEM((16, 128, 128), BF16),
+            pltpu.VMEM((16, 128), F32),
+            pltpu.VMEM((8, 128), F32),
+            pltpu.VMEM((8, 128), F32),
         ),
         in_specs=[hbm] * 10,
-        out_specs=(hbm,) * 6,
+        out_specs=(vm,) * 6,
         scratch_shapes=list(SCRATCH),
         compiler_params=pltpu.CompilerParams(
-            collective_id=0, has_side_effects=True, vmem_limit_bytes=62 * 1024 * 1024),
+            collective_id=0, has_side_effects=True, vmem_limit_bytes=54 * 1024 * 1024),
         name="fused",
     )(tokens, va, ga, cot, vw, gw, mixw, gain, bias, mixb)
 
 
-def finish(tgrad, wsum, mixs, bsum, nsum, hsum, tout, vout, gout, mout, bout, nout, hout,
-           tbuf, wbuf, wide, mbuf, mwide, bbuf, nbuf, hbuf, isem, osem):
-    small = ((bsum, bbuf, bout), (nsum, nbuf, nout), (hsum, hbuf, hout))
-    gets = [pltpu.make_async_copy(wsum.at[0], wbuf.at[0], isem.at[0]), pltpu.make_async_copy(wsum.at[1], wbuf.at[1], isem.at[1]),
-            pltpu.make_async_copy(mixs, mbuf, isem.at[2])]
-    puts = [pltpu.make_async_copy(wide.at[0], vout, osem.at[0]), pltpu.make_async_copy(wide.at[1], gout, osem.at[1]),
-            pltpu.make_async_copy(mwide, mout, osem.at[2])]
-    for k, (src, buf, dst) in enumerate(small):
-        gets.append(pltpu.make_async_copy(src, buf, isem.at[3 + k]))
-        puts.append(pltpu.make_async_copy(buf, dst, osem.at[3 + k]))
-    for k in range(4):
-        rows = pl.ds(k * 96, 96)
-        gets.append(pltpu.make_async_copy(tgrad.at[rows], tbuf.at[rows], isem.at[6 + k]))
-        puts.append(pltpu.make_async_copy(tbuf.at[rows], tout.at[rows], osem.at[6 + k]))
-    for get in gets:
-        get.start()
+def finish(tgrad, wsum, mixs, bsum, nsum, hsum, tout, vout, gout, mout, bout, nout, hout, wide, mwide, osem):
+    pairs = [(tgrad, tout), (wide.at[0], vout), (wide.at[1], gout), (mwide, mout), (bsum, bout), (nsum, nout), (hsum, hout)]
+    puts = [pltpu.make_async_copy(src, dst, osem.at[k]) for k, (src, dst) in enumerate(pairs)]
+    for k in (0, 4, 5, 6):
+        puts[k].start()
     for k in range(2):
-        gets[k].wait()
-        wide[k] = wbuf[k].astype(F32)
-        puts[k].start()
-    gets[2].wait()
-    mwide[...] = mbuf[...].astype(F32)
-    puts[2].start()
-    for k in range(3, 10):
-        gets[k].wait()
-        puts[k].start()
+        wide[k] = wsum[k].astype(F32)
+        puts[1 + k].start()
+    mwide[...] = mixs[...].astype(F32)
+    puts[3].start()
     for put in puts:
         put.wait()
 
 
 def finish_call(*parts):
-    hbm = pl.BlockSpec(memory_space=pl.ANY)
+    hbm = pl.BlockSpec(memory_space=pltpu.HBM)
+    vm = pl.BlockSpec(memory_space=pltpu.VMEM)
     return pl.pallas_call(
         finish,
         out_shape=(
@@ -792,20 +795,14 @@
             jax.ShapeDtypeStruct((8, 128), F32),
             jax.ShapeDtypeStruct((8, 128), F32),
         ),
-        in_specs=[hbm] * 6,
+        in_specs=[vm] * 6,
         out_specs=(hbm,) * 7,
         scratch_shapes=[
-            pltpu.VMEM((384, 2048), BF16),
-            pltpu.VMEM((2, 128, 1024), BF16),
             pltpu.VMEM((2, 128, 1024), F32),
-            pltpu.VMEM((16, 128, 128), BF16),
             pltpu.VMEM((16, 128, 128), F32),
-            pltpu.VMEM((16, 128), F32),
-            pltpu.VMEM((8, 128), F32),
-            pltpu.VMEM((8, 128), F32),
-            pltpu.SemaphoreType.DMA((10,)),
-            pltpu.SemaphoreType.DMA((10,)),
+            pltpu.SemaphoreType.DMA((7,)),
         ],
+        compiler_params=pltpu.CompilerParams(vmem_limit_bytes=16 * 1024 * 1024),
         name="finish",
     )(*parts)
 

time: 75.5 us -> 65.8 us (0.87)
  Pallas kernels: 74.7 us -> 64.9 us
    pallas_call x1, Pallas kernels: 71.7 us -> 63 us  [fused_call(): pl.pallas_call(fused, out_shape=(pltpu.VMEM((384, 2048), BF16), pltpu.VME...]
    pallas_call x1, Pallas kernels: 3 us -> 1.91 us  [finish_call(): pl.pallas_call(finish, out_shape=(jax.ShapeDtypeStruct((384, 2048), BF16)...]
where the time goes in v3:
time: 65.8 us; the launch traced here: 65.7 us
  Pallas kernels  64.9 us (99%)
  between operations  0.8 us (1%)
    pallas_call x1, Pallas kernels, fused_call(): pl.pallas_call(fused, out_shape=(pltpu.VMEM((384, 2048), BF16), pltpu.VME...  63 us
    pallas_call x1, Pallas kernels, finish_call(): pl.pallas_call(finish, out_shape=(jax.ShapeDtypeStruct((384, 2048), BF16)...  1.91 us

profile of v3, /device:TPU:1, one launch (start us, length us, event | category | flops | bytes accessed | tf_op | source)
XLA Modules:
  0.0 65.7 jit_solution(15574902287600796844)
XLA Ops:
  0.6 63.0 %fused.1 = (bf16[384,2048]{1,0:T(8,128)(2,1)S(1)}, bf16[2,128,1024]{2,1,0:T(8,128)(2,1)S(1)}, bf16[16,128,128]{2,1,0:T(8,128)(2,1)S(1)}, f32[16,128]{1,0:T(8,128...) custom-call(bf16[384,2048]{1,0:T(8,128)(2,1)} %bitcast.9, bf16[384,1024]{1,0:T(8,128)(2,1)} %bitcast.10, ...), custom_call_target="tpu_custom_call" | custom-call | tf_op jit(solution)/shard_map/fused/pallas_call | solution.py:751
  63.6 1.9 %finish.1 = (bf16[384,2048]{1,0:T(8,128)(2,1)}, f32[128,1024]{1,0:T(8,128)}, f32[128,1024]{1,0:T(8,128)}, f32[16,128,128]{2,1,0:T(8,128)}, f32[16,128]{1,0:T(8,1...) custom-call(bf16[384,2048]{1,0:T(8,128)(2,1)S(1)} %get-tuple-element.20.tgrad, ...), custom_call_target="tpu_custom_call" | custom-call | tf_op jit(solution)/shard_map/finish/pallas_call | solution.py:787

commit v4 on v3

--- a/solution.py
+++ b/solution.py
@@ -275,13 +275,6 @@
 
     lax.fori_loop(0, 24 // GATE_UNROLL, second, 0)
 
-    mark("transpose")
-    for k in range(8):
-        local[5 + k].wait()
-        tt[k * 128:(k + 1) * 128, 0:384] = tokl[k].T
-    await_recv(tokr, tok_s.at[0], tok_r.at[0])
-    for k in range(8):
-        tt[k * 128:(k + 1) * 128, 384:768] = tokr[k].T
     mark("help1")
     for v in range(2):
         ring_part(1, v, 1)
@@ -350,6 +343,13 @@
     lax.fori_loop(0, 24 // LAST_UNROLL, last, 0)
     for j in range(4):
         swap(1, j).start()
+    mark("transpose")
+    for k in range(8):
+        local[5 + k].wait()
+        tt[k * 128:(k + 1) * 128, 0:384] = tokl[k].T
+    await_recv(tokr, tok_s.at[0], tok_r.at[0])
+    for k in range(8):
+        tt[k * 128:(k + 1) * 128, 384:768] = tokr[k].T
     def stats_pair():
         mark("m_stats")
         parts = split3(gsum[...])
@@ -466,14 +466,18 @@
             mq[k] = v
             mqb[k] = v.astype(BF16)
         for k in range(1, 4):
-            copy(mqb.at[:, lax.rem(x + k, 4)], mr1.at[k - 1], mix_s.at[1], mix_r.at[1], along("x", k)).start()
+            for h in range(2):
+                copy(mqb.at[pl.ds(4 * h, 4), lax.rem(place[h] + k, 4)], mr1.at[k - 1, pl.ds(4 * h, 4)],
+                     mix_s.at[1], mix_r.at[1], along(axes[h], k)).start()
 
     def mix_z():
         mark("mix_z")
         await_recv(mr1, mix_s.at[1], mix_r.at[1])
-        v = mq[:, x] + (mr1[0].astype(F32) + mr1[1].astype(F32)) + mr1[2].astype(F32)
-        mq1[...] = v
-        mq1b[...] = v.astype(BF16)
+        for h in range(2):
+            r = slice(4 * h, 4 * h + 4)
+            v = mq[r, place[h]] + (mr1[0, r].astype(F32) + mr1[1, r].astype(F32)) + mr1[2, r].astype(F32)
+            mq1[r] = v
+            mq1b[r] = v.astype(BF16)
         for k in range(1, 8):
             copy(mq1b.at[lax.rem(z + k, 8)], mr2.at[k - 1], mix_s.at[2], mix_r.at[2], along("z", k)).start()
 
@@ -484,9 +488,12 @@
         for k in range(7):
             v = v + mr2[k].astype(F32)
         mpart[...] = v
-        my[y] = v
+        on_x = z // 4
+        slot = y * (1 - on_x) + x * on_x
+        my[slot] = v
         for k in range(1, 4):
-            copy(mpart, my.at[y], mix_s.at[3], mix_r.at[3], along("y", k)).start()
+            to = at(nx=lax.rem(x + k * on_x, 4), ny=lax.rem(y + k * (1 - on_x), 4))
+            copy(mpart, my.at[slot], mix_s.at[3], mix_r.at[3], to).start()
 
     def mix_back_z():
         mark("mix_back_z")
@@ -500,9 +507,11 @@
     def mix_back_x():
         mark("mix_back_x")
         await_recv(maz.at[pl.ds(0, 7)], mix_s.at[4], mix_r.at[4])
-        max_[x] = maz[...]
-        for k in range(1, 4):
-            copy(maz, max_.at[x], mix_s.at[5], mix_r.at[5], along("x", k)).start()
+        for h in range(2):
+            r = pl.ds(4 * h, 4)
+            max_[place[h], r] = maz[r]
+            for k in range(1, 4):
+                copy(maz.at[r], max_.at[place[h], r], mix_s.at[5], mix_r.at[5], along(axes[h], k)).start()
 
     def mix_back_c():
         mark("mix_back_c")
@@ -564,7 +573,7 @@
             v = v + r3[g, k].astype(F32)
         fin[g] = v.astype(BF16)
         allf[g, sp] = v.astype(BF16)
-        for k in range(1, 16):
+        for k in (10, 6, 9, 11, 14, 2, 5, 7, 8, 13, 15, 1, 3, 4, 12):
             copy(fin.at[g], allf.at[g, sp], fou_s.at[g], fou_r.at[g], {"sp": lax.rem(sp + k, 16), "dp": dp}).start()
 
     def stage_end(g):
@@ -576,10 +585,10 @@
             wout[h, a * 32:(a + 1) * 32, b * 256 + n * 128:b * 256 + (n + 1) * 128] = allf[g, s]
 
     far_tiles(0)
+    far_tiles(1)
     ring(1, 0)
     mix_x()
     stats_pair()
-    far_tiles(1)
     near_tiles(0)
     ring(1, 1)
     near_tiles(1)
@@ -593,7 +602,6 @@
     into(0)
     mix_z()
     into(1)
-    stats_y()
     ring(2, 1)
     stage_two(0)
     ring(3, 0)
@@ -601,8 +609,8 @@
     mix_y()
     stage_two(1)
     stage_two(3)
+    stats_y()
     ring(3, 1)
-    stats_z()
     for v in range(2):
         help_out(2, v)
     mix_back_z()
@@ -610,6 +618,7 @@
     stage_three(2)
     stage_three(1)
     stage_three(3)
+    stats_z()
     ring(4, 0)
     ring(4, 1)
     for v in range(2):
@@ -622,11 +631,11 @@
     stage_four(2)
     stage_four(1)
     stage_four(3)
-    stats_back()
-    into(2)
     mark("help_pair3")
     help_pair(3)
     help_pair(4)
+    into(2)
+    stats_back()
     into(3)
     mix_back_c()
     into(4)

time: 65.8 us -> 65.7 us (level)
  no operation moved by 1% of the time
where the time goes in v4:
time: 65.7 us; the launch traced here: 65.4 us
  Pallas kernels  64.6 us (98%)
  between operations  0.8 us (1%)
    pallas_call x1, Pallas kernels, fused_call(): pl.pallas_call(fused, out_shape=(pltpu.VMEM((384, 2048), BF16), pltpu.VME...  62.7 us
    pallas_call x1, Pallas kernels, finish_call(): pl.pallas_call(finish, out_shape=(jax.ShapeDtypeStruct((384, 2048), BF16)...  1.91 us

profile of v4, /device:TPU:1, one launch (start us, length us, event | category | flops | bytes accessed | tf_op | source)
XLA Modules:
  0.0 65.4 jit_solution(16191695086802726524)
XLA Ops:
  0.6 62.7 %fused.1 = (bf16[384,2048]{1,0:T(8,128)(2,1)S(1)}, bf16[2,128,1024]{2,1,0:T(8,128)(2,1)S(1)}, bf16[16,128,128]{2,1,0:T(8,128)(2,1)S(1)}, f32[16,128]{1,0:T(8,128...) custom-call(bf16[384,2048]{1,0:T(8,128)(2,1)} %bitcast.9, bf16[384,1024]{1,0:T(8,128)(2,1)} %bitcast.10, ...), custom_call_target="tpu_custom_call" | custom-call | tf_op jit(solution)/shard_map/fused/pallas_call | solution.py:760
  63.4 1.9 %finish.1 = (bf16[384,2048]{1,0:T(8,128)(2,1)}, f32[128,1024]{1,0:T(8,128)}, f32[128,1024]{1,0:T(8,128)}, f32[16,128,128]{2,1,0:T(8,128)}, f32[16,128]{1,0:T(8,1...) custom-call(bf16[384,2048]{1,0:T(8,128)(2,1)S(1)} %get-tuple-element.20.tgrad, ...), custom_call_target="tpu_custom_call" | custom-call | tf_op jit(solution)/shard_map/finish/pallas_call | solution.py:796
